TPU v7x, 32 devices: a whole 2x2x4 slice. The times are simulated.
32 devices in a mesh: sp: 4 (over z), fs: 4 (over y, x), tp: 2 (over core).
Axes of the slice: x: 2, y: 2, z: 4, core: 2. Of those that a mesh axis runs over, the one named last changes fastest.
Arguments:
- tokens: bfloat16 [4, 1024, 2048], P('fs', 'sp', 'tp'), may hold values from -6 to 6
- norm_gain: float32 [2048], replicated, may hold values from 0.1 to 1.9
- lin_query: bfloat16 [2048, 1024], P(None, ('fs', 'tp')), may hold values from -0.125 to 0.125
- lin_key: bfloat16 [2048, 1024], P(None, ('fs', 'tp')), may hold values from -0.125 to 0.125
- lin_value: bfloat16 [2048, 2048], P(None, ('fs', 'tp')), may hold values from -0.125 to 0.125
- lin_decay: bfloat16 [2048, 1024], P(None, ('fs', 'tp')), may hold values from -0.125 to 0.125
- decay_bias: float32 [1024], replicated, may hold values from -0.5 to 8.5
- decay_shift: bfloat16 [2, 4, 1024], P(None, 'fs', 'sp'), may hold values from -1.4 to 1.5, as said below
- soft_query: bfloat16 [2048, 2048], P(None, ('fs', 'tp')), may hold values from -0.190034947 to 0.190034947
- soft_key: bfloat16 [2048, 2048], P(None, ('fs', 'tp')), may hold values from -1.9887378 to 1.9887378
- soft_value: bfloat16 [2048, 2048], P(None, ('fs', 'tp')), may hold values from -0.125 to 0.125
- soft_lambda: float32 [8], replicated, may hold values from 0.3 to 0.8
- lin_gain: float32 [256], replicated, may hold values from 0.1 to 1.9
- soft_gain: float32 [256], replicated, may hold values from 0.1 to 1.9
- lin_out: bfloat16 [2048, 2048], P(('fs', 'tp')), may hold values from -0.09375 to 0.09375
- soft_out: bfloat16 [2048, 2048], P(('fs', 'tp')), may hold values from -0.09375 to 0.09375
Outputs:
- mixed: bfloat16 [4, 1024, 2048], P('fs', 'sp', 'tp')
- log_mass: float32 [8, 2, 4, 1024], P(('fs', 'tp'), None, None, 'sp')
Inputs may be any that keep to these rules, and one draw needn't show every extreme that they name: `decay_shift`: row 1 is never positive.
All inputs are finite; a program needn't handle non-finite values.
Results may differ from a plain program's by a relative error of at most 0.02.
Values may be sent and summed in bfloat16 or wider, within the bound.
A program may use at most 192 MiB of HBM per device.

v0:
```python
import functools

import jax
import jax.numpy as jnp
import numpy as np
from jax import lax
from jax.experimental import pallas as pl
from jax.experimental.pallas import tpu as pltpu
from jax.sharding import PartitionSpec as P

GLA_KEY = 128
GLA_VALUE = 256
DIFF_HEAD = 128
DIFF_VALUE = 256
BLOCK = 64


norm_eps = 1e-06
decay_tau = 16.0
rope_base = 500000.0
highest = lax.Precision.HIGHEST


def prefix(array, axis, join, neutral):
    place = lax.axis_index(axis)
    gathered = jax.tree.map(
        lambda a, kind: lax.all_gather(a.astype(kind), axis), array, (jnp.bfloat16, jnp.bfloat16)
    )
    state = jax.tree.map(lambda a, e: jnp.zeros_like(a) + jnp.asarray(e, a.dtype), array, neutral)

    def one(turn, state):
        return join(
            state,
            jax.tree.map(
                lambda a, own: lax.dynamic_index_in_dim(a, turn, 0, False).astype(own.dtype),
                gathered,
                array,
            ),
        )

    return lax.fori_loop(0, place, one, state)


def scaled_rms(values, norm_gain):
    return (
        values * lax.rsqrt(jnp.mean(values * values, axis=-1, keepdims=True) + norm_eps) * norm_gain
    )


def rotate(values, positions):
    half_dim = values.shape[-1] // 2
    inv_freq = jnp.power(
        jnp.float32(rope_base), -jnp.arange(half_dim, dtype=jnp.float32) * (2.0 / values.shape[-1])
    )
    angles = positions.astype(jnp.float32)[:, None] * inv_freq[None, :]
    cos_table = jnp.cos(angles)[:, None, None, :]
    sin_table = jnp.sin(angles)[:, None, None, :]
    widened = values.astype(jnp.float32)
    first_half = widened[..., :half_dim]
    second_half = widened[..., half_dim:]
    turned = jnp.concatenate(
        [
            first_half * cos_table - second_half * sin_table,
            second_half * cos_table + first_half * sin_table,
        ],
        axis=-1,
    )
    return turned.astype(jnp.bfloat16)


def block_pass(queries, key_rows, value_rows, log_decay, block_len):
    groups, length, heads, key_dim = queries.shape
    value_dim = value_rows.shape[-1]
    block_count = length // block_len

    def split(tensor):
        return tensor.reshape(groups, block_count, block_len, heads, tensor.shape[-1]).transpose(
            1, 0, 3, 2, 4
        )

    causal = jnp.tril(jnp.ones((block_len, block_len), dtype=bool))[:, :, None]

    def advance(carry, inputs):
        state_now, offset = carry
        query_blk, key_blk, value_blk, decay_blk = inputs
        cum_log = jnp.cumsum(decay_blk, axis=2)
        inner_part = jnp.einsum(
            "bhcd,bhdv->bhcv", query_blk * jnp.exp(cum_log), state_now, precision=highest
        )
        decay_pair = jnp.exp(
            jnp.where(causal, cum_log[:, :, :, None, :] - cum_log[:, :, None, :, :], -jnp.inf)
        )
        scores = jnp.sum(
            query_blk[:, :, :, None, :] * key_blk[:, :, None, :, :] * decay_pair, axis=-1
        )
        local_part = jnp.einsum("bhij,bhjv->bhiv", scores, value_blk, precision=highest)
        last_log = cum_log[:, :, -1, :]
        state_now = jnp.exp(last_log)[..., None] * state_now + jnp.einsum(
            "bhcd,bhcv->bhdv",
            key_blk * jnp.exp(last_log[:, :, None, :] - cum_log),
            value_blk,
            precision=highest,
        )
        carried = query_blk * jnp.exp(offset[:, :, None, :] + cum_log)
        return ((state_now, offset + last_log), (inner_part + local_part, carried))

    start = (
        jnp.zeros((groups, heads, key_dim, value_dim), jnp.float32),
        jnp.zeros((groups, heads, key_dim), jnp.float32),
    )
    (state_end, offset_end), (outs, carried) = lax.scan(
        advance, start, (split(queries), split(key_rows), split(value_rows), split(log_decay))
    )
    return (outs, carried, state_end, offset_end)


def project(rows, weight):
    lead_shape = rows.shape[:-1]
    flat_rows = rows.reshape(-1, rows.shape[-1])
    product = jnp.dot(flat_rows, weight, preferred_element_type=jnp.float32)
    return product.reshape(lead_shape + (weight.shape[1],))


def chain_join(earlier, later):
    return (earlier[0] * later[0], later[0][..., None] * earlier[1] + later[1])


def attend(queries, query_pos, reach, all_keys, all_values, soft_lambda, soft_gain, rows_dev):
    groups, query_rows, soft_heads = queries.shape[:3]
    block_total = all_keys.shape[1] // rows_dev
    scale = DIFF_HEAD ** (-0.5)

    def first_pass(block_id, carry):
        top_now, total_now, score_store = carry
        key_blk = lax.dynamic_slice_in_dim(all_keys, block_id * rows_dev, rows_dev, 1)
        raw_scores = (
            jnp.einsum("bqhmd,bkhmd->bhmqk", queries, key_blk, preferred_element_type=jnp.float32)
            * scale
        )
        key_pos = block_id * rows_dev + jnp.arange(rows_dev, dtype=jnp.int32)
        scores = jnp.where(key_pos[None, :] <= query_pos[:, None], raw_scores, -jnp.inf)
        top_next = jnp.maximum(top_now, jnp.max(scores, axis=-1))
        total_next = total_now * jnp.exp(top_now - top_next) + jnp.sum(
            jnp.exp(scores - top_next[..., None]), axis=-1
        )
        score_store = lax.dynamic_update_index_in_dim(score_store, scores, block_id, 0)
        return (top_next, total_next, score_store)

    stat_shape = (groups, soft_heads, 2, query_rows)
    store_init = jnp.full((block_total,) + stat_shape + (rows_dev,), -jnp.inf, jnp.float32)
    top_all, total_all, score_store = lax.fori_loop(
        0,
        reach,
        first_pass,
        (
            jnp.full(stat_shape, -jnp.inf, jnp.float32),
            jnp.zeros(stat_shape, jnp.float32),
            store_init,
        ),
    )
    mass = top_all + jnp.log(total_all)

    def second_pass(block_id, accum):
        scores = lax.dynamic_index_in_dim(score_store, block_id, 0, keepdims=False)
        probs = jnp.exp(scores - top_all[..., None]) / total_all[..., None]
        weights = (probs[:, :, 0] - soft_lambda[None, :, None, None] * probs[:, :, 1]).astype(
            jnp.bfloat16
        )
        value_blk = lax.dynamic_slice_in_dim(all_values, block_id * rows_dev, rows_dev, 1)
        return accum + jnp.einsum(
            "bhqk,bkhv->bhqv", weights, value_blk, preferred_element_type=jnp.float32
        )

    accum = lax.fori_loop(
        0, reach, second_pass, jnp.zeros((groups, soft_heads, query_rows, DIFF_VALUE), jnp.float32)
    )
    soft_mix = scaled_rms(accum, soft_gain).astype(jnp.bfloat16).transpose(0, 2, 1, 3)
    soft_mix = soft_mix.reshape(groups, query_rows, soft_heads * DIFF_VALUE)
    return (soft_mix, mass)


def mixers(
    normed,
    shift_rows,
    lin_query,
    lin_key,
    lin_value,
    lin_decay,
    decay_bias,
    soft_query,
    soft_key,
    soft_value,
    soft_lambda,
    lin_gain,
    soft_gain,
):
    groups, rows_dev, model_width = normed.shape
    lin_heads = lin_query.shape[1] // GLA_KEY
    soft_heads = soft_value.shape[1] // DIFF_VALUE
    place = lax.axis_index("sp")
    shift_wide = shift_rows.astype(jnp.float32)
    lin_q = (
        project(normed, lin_query)
        .astype(jnp.bfloat16)
        .reshape(groups, rows_dev, lin_heads, GLA_KEY)
    )
    lin_k = (
        project(normed, lin_key).astype(jnp.bfloat16).reshape(groups, rows_dev, lin_heads, GLA_KEY)
    )
    lin_v = (
        project(normed, lin_value)
        .astype(jnp.bfloat16)
        .reshape(groups, rows_dev, lin_heads, GLA_VALUE)
    )
    gate_input = project(normed, lin_decay) + decay_bias + shift_wide[0][:, :, None]
    log_decay = jax.nn.log_sigmoid(gate_input) / decay_tau + shift_wide[1][:, :, None]
    log_decay = log_decay.reshape(groups, rows_dev, lin_heads, GLA_KEY)
    outs, carried, state_end, offset_end = block_pass(
        lin_q.astype(jnp.float32),
        lin_k.astype(jnp.float32),
        lin_v.astype(jnp.float32),
        log_decay,
        BLOCK,
    )
    keep_in, state_in = prefix(
        (jnp.exp(offset_end), state_end),
        "sp",
        chain_join,
        (jnp.ones_like(offset_end), jnp.zeros_like(state_end)),
    )
    outs = outs + jnp.einsum("nbhcd,bhdv->nbhcv", carried, state_in, precision=highest)
    lin_raw = outs.transpose(1, 0, 3, 2, 4).reshape(groups, rows_dev, lin_heads, GLA_VALUE)
    lin_mix = (
        scaled_rms(lin_raw, lin_gain)
        .astype(jnp.bfloat16)
        .reshape(groups, rows_dev, lin_heads * GLA_VALUE)
    )
    positions = place * rows_dev + jnp.arange(rows_dev, dtype=jnp.int32)
    soft_q = rotate(
        project(normed, soft_query)
        .astype(jnp.bfloat16)
        .reshape(groups, rows_dev, soft_heads, 2, DIFF_HEAD),
        positions,
    )
    soft_k = rotate(
        project(normed, soft_key)
        .astype(jnp.bfloat16)
        .reshape(groups, rows_dev, soft_heads, 2, DIFF_HEAD),
        positions,
    )
    soft_v = (
        project(normed, soft_value)
        .astype(jnp.bfloat16)
        .reshape(groups, rows_dev, soft_heads, DIFF_VALUE)
    )
    all_keys, all_values = (
        lax.all_gather(soft_k, "sp", axis=1, tiled=True),
        lax.all_gather(soft_v, "sp", axis=1, tiled=True),
    )
    soft_mix, mass = attend(
        soft_q, positions, place + 1, all_keys, all_values, soft_lambda, soft_gain, rows_dev
    )
    return (lin_mix, soft_mix, mass)


def output_term(lin_mix, soft_mix, lin_out, soft_out, rows_dev, parts):
    col_width = lin_out.shape[1] // parts

    def term(start, row_count):
        pieces = []
        for turn_index in range(row_count // rows_dev):
            piece_id = (start + turn_index * rows_dev) // rows_dev
            seq_id = piece_id // parts
            part_id = piece_id % parts
            lin_rows = lax.dynamic_index_in_dim(lin_mix, seq_id, 0, keepdims=False)
            soft_rows = lax.dynamic_index_in_dim(soft_mix, seq_id, 0, keepdims=False)
            lin_cols = lax.dynamic_slice_in_dim(lin_out, part_id * col_width, col_width, 1)
            soft_cols = lax.dynamic_slice_in_dim(soft_out, part_id * col_width, col_width, 1)
            pieces.append(
                jnp.dot(lin_rows, lin_cols, preferred_element_type=jnp.float32)
                + jnp.dot(soft_rows, soft_cols, preferred_element_type=jnp.float32)
            )
        return jnp.concatenate(pieces, axis=0)

    return term


def shards(
    tokens,
    norm_gain,
    lin_query,
    lin_key,
    lin_value,
    lin_decay,
    decay_bias,
    decay_shift,
    soft_query,
    soft_key,
    soft_value,
    soft_lambda,
    lin_gain,
    soft_gain,
    lin_out,
    soft_out,
):
    rows_dev = tokens.shape[1]
    parts = lax.axis_size("tp")
    fs_size = lax.axis_size("fs")
    fs_index = lax.axis_index("fs")
    tp_index = lax.axis_index("tp")
    whole = lax.all_gather(tokens, "tp", axis=2, tiled=True).astype(jnp.float32)
    normed = scaled_rms(whole, norm_gain).astype(jnp.bfloat16)
    lambda_grid = soft_lambda.reshape(fs_size, parts, -1)
    bias_grid = decay_bias.reshape(fs_size, parts, -1)
    all_rows, all_shift = (
        lax.all_gather(normed, "fs", axis=0, tiled=True),
        lax.all_gather(decay_shift, "fs", axis=1, tiled=True),
    )
    head_lambda = lax.dynamic_index_in_dim(
        lax.dynamic_index_in_dim(lambda_grid, fs_index, 0, keepdims=False),
        tp_index,
        0,
        keepdims=False,
    )
    head_bias = lax.dynamic_index_in_dim(
        lax.dynamic_index_in_dim(bias_grid, fs_index, 0, keepdims=False),
        tp_index,
        0,
        keepdims=False,
    )
    lin_mix, soft_mix, mass = mixers(
        all_rows,
        all_shift,
        lin_query,
        lin_key,
        lin_value,
        lin_decay,
        head_bias,
        soft_query,
        soft_key,
        soft_value,
        head_lambda,
        lin_gain,
        soft_gain,
    )
    term = output_term(lin_mix, soft_mix, lin_out, soft_out, rows_dev, parts)
    summed = lax.psum_scatter(
        term(jnp.int32(0), rows_dev * lax.axis_size(("fs", "tp"))).astype(jnp.bfloat16),
        ("fs", "tp"),
        scatter_dimension=0,
        tiled=True,
    ).astype(jnp.float32)
    log_mass = mass.transpose(1, 2, 0, 3)
    mixed = summed.astype(jnp.bfloat16).reshape(1, rows_dev, summed.shape[1])
    return (mixed, log_mass)


CHUNK = 128


def level_sums(length):
    levels = length.bit_length() - 1
    row = np.arange(length)
    spans = []
    for level in range(levels):
        half = 1 << level
        middle = (row // (2 * half)) * (2 * half) + half - 1
        low, high = np.minimum(row, middle), np.maximum(row, middle)
        spans.append((row[None, :] > low[:, None]) & (row[None, :] <= high[:, None]))
    spans.append(row[None, :] <= row[:, None])
    spans.append(row[None, :] > row[:, None])
    table = np.concatenate(spans, axis=0)
    return np.concatenate([table, table], axis=1).astype(np.float32)


def turn_tables(length):
    half = DIFF_HEAD // 2
    inv_freq = rope_base ** (-np.arange(half, dtype=np.float64) * (2.0 / DIFF_HEAD))
    angles = np.arange(length, dtype=np.float64)[:, None] * inv_freq[None, :]
    cos, sin = np.cos(angles), np.sin(angles)
    return (
        np.concatenate([cos, cos], axis=1).astype(np.float32),
        np.concatenate([-sin, sin], axis=1).astype(np.float32),
    )


def nt(a, b):
    return lax.dot_general(a, b, (((1,), (1,)), ((), ())), preferred_element_type=jnp.float32)


def tn(a, b):
    return lax.dot_general(a, b, (((0,), (0,)), ((), ())), preferred_element_type=jnp.float32)


def nn(a, b):
    return jnp.dot(a, b, preferred_element_type=jnp.float32)


WEIGHTS = 12


def layer_kernel(
    sizes,
    tok_ref, shift_ref, gain_ref, bias_ref, lam_ref, lgain_ref, sgain_ref, *refs,
):
    far = refs[:WEIGHTS]
    out_ref, all_mass_ref = refs[WEIGHTS : WEIGHTS + 2]
    near = refs[WEIGHTS + 2 : 2 * WEIGHTS + 2]
    (
        x_ref, rows_ref, q_s, k_s, v_s, dec_s, a_s, b_s, c_s, state_s, lmix_s, smix_s,
        part_ref, mass_ref, pair, held, landing, final, via,
        wsem, via_send, via_recv, in_send1, in_recv1, in_send2, in_recv2, in_send3, in_recv3, ssend, srecv,
        send1, recv1, send2, recv2, send3, recv3, msend, mrecv,
    ) = refs[2 * WEIGHTS + 2 :]
    lq_ref, lk_ref, ld_ref, lv_ref, cos_ref, sin_ref, sq_ref, sk_ref, sv_ref, span_ref, lo_ref, so_ref = near
    planes, count, parts, piece, width = x_ref.shape
    rows = count * piece
    scale = DIFF_HEAD ** (-0.5)
    bf = jnp.bfloat16
    me_sp, me_fs, me_tp = lax.axis_index("sp"), lax.axis_index("fs"), lax.axis_index("tp")
    other = 1 - me_tp
    home = me_sp == me_fs

    def remote(src, dst, send, recv, sp, fs, tp):
        return pltpu.make_async_remote_copy(
            src_ref=src,
            dst_ref=dst,
            send_sem=send,
            recv_sem=recv,
            device_id={"sp": sp, "fs": fs, "tp": tp},
            device_id_type=pl.DeviceIdType.MESH,
        )

    def landed(ref, sem):
        pltpu.make_async_copy(ref, ref, sem).wait()

    def rows_out(c):
        return remote(
            tok_ref.at[pl.ds(c * piece, piece)], via.at[me_fs],
            via_send.at[c], via_recv.at[me_fs], me_sp, c, me_tp,
        )

    def rows_on(z):
        return remote(
            via.at[z], x_ref.at[me_sp, me_fs, me_tp],
            in_send1.at[z], in_recv1.at[me_sp], z, me_fs, me_tp,
        )

    def shifts_out(c):
        return remote(
            shift_ref, rows_ref.at[me_sp], ssend.at[c], srecv.at[me_sp], me_fs, c, me_tp
        )

    def spread(p, d):
        block = x_ref.at[p, me_fs, me_tp]
        return remote(
            block, block, in_send2.at[p, d], in_recv2.at[p, d],
            me_sp, lax.rem(me_fs + d, count), me_tp,
        )

    def source(d):
        return lax.rem(me_fs + count - d, count)

    def across(p, d):
        block = x_ref.at[p, source(d), me_tp]
        return remote(block, block, in_send3.at[p, d], in_recv3.at[p, d], me_sp, me_fs, other)

    def pair_out(p):
        return remote(
            part_ref.at[other, p], pair.at[p], send1.at[p], recv1.at[p], me_sp, me_fs, other
        )

    def plane_out(p, d):
        c = lax.rem(me_fs + d, count)
        return remote(
            held.at[p, c], landing.at[p, d - 1], send2.at[p, d], recv2.at[p, d], me_sp, c, me_tp
        )

    def home_out(p):
        return remote(
            final.at[p], out_ref.at[me_fs], send3.at[p], recv3.at[me_fs], p, me_sp, me_tp
        )

    def mass_out(p):
        return remote(
            mass_ref.at[p], all_mass_ref.at[me_sp], msend.at[p], mrecv.at[me_sp], p, me_fs, me_tp
        )

    def mine(p):
        return jnp.logical_and(home, p == me_sp)

    loads = [pltpu.make_async_copy(f, n, wsem.at[i]) for i, (f, n) in enumerate(zip(far, near))]

    for d in range(1, count):
        rows_out(lax.rem(me_fs + d, count)).start()
    pltpu.make_async_copy(
        tok_ref.at[pl.ds(me_fs * piece, piece)], via.at[me_fs], via_recv.at[me_fs]
    ).start()
    for c in range(count):
        own = jnp.logical_and(home, c == me_fs)

        @pl.when(jnp.logical_not(own))
        def _():
            shifts_out(c).start()

        @pl.when(own)
        def _():
            pltpu.make_async_copy(shift_ref, rows_ref.at[me_sp], srecv.at[me_sp]).start()

    for d in range(count):
        z = lax.rem(me_fs + d, count)
        landed(via.at[z], via_recv.at[z])

        @pl.when(z != me_sp)
        def _():
            rows_on(z).start()

        @pl.when(z == me_sp)
        def _():
            pltpu.make_async_copy(
                via.at[z], x_ref.at[me_sp, me_fs, me_tp], in_recv1.at[me_sp]
            ).start()

    for load in loads:
        load.start()

    def arrive(p):
        landed(x_ref.at[p, me_fs, me_tp], in_recv1.at[p])
        for d in range(1, count):
            spread(p, d).start()
        across(p, 0).start()

    def relay(p):
        for d in range(1, count):
            landed(x_ref.at[p, source(d), me_tp], in_recv2.at[p, d])
            across(p, d).start()

    def complete(p):
        for d in range(count):
            landed(x_ref.at[p, source(d), other], in_recv3.at[p, d])
        landed(rows_ref.at[p], srecv.at[p])

    def project_rows(p):
        here = pl.ds(p * rows, rows)
        halves = [x_ref[p, :, t].reshape(rows, width).astype(jnp.float32) for t in range(parts)]
        square = sum(jnp.sum(h * h, axis=-1, keepdims=True) for h in halves)
        factor = lax.rsqrt(square / (parts * width) + norm_eps)
        normed = jnp.concatenate(
            [
                (h * factor * gain_ref[:, t * width : (t + 1) * width]).astype(bf)
                for t, h in enumerate(halves)
            ],
            axis=1,
        )
        qk = nn(normed, jnp.concatenate([lq_ref[...], lk_ref[...]], axis=1)).astype(bf)
        q_s[here, :] = qk[:, :GLA_KEY]
        k_s[here, :] = qk[:, GLA_KEY:]
        v_s[here, :] = nn(normed, lv_ref[...]).astype(bf)
        lane = lax.broadcasted_iota(jnp.int32, (rows_ref.shape[1], 2 * GLA_KEY), 1)
        sub = lax.broadcasted_iota(jnp.int32, (rows_ref.shape[1], 2 * GLA_KEY), 0)
        pick = jnp.where(sub == lane // GLA_KEY, 1.0, 0.0).astype(bf)
        shift = tn(rows_ref[p], pick)
        gate = nn(normed, ld_ref[...]) + bias_ref[...] + shift[:, :GLA_KEY]
        log_sig = jnp.minimum(gate, 0.0) - jnp.log1p(jnp.exp(-jnp.abs(gate)))
        dec_s[here, :] = log_sig * (1.0 / decay_tau) + shift[:, GLA_KEY:]
        cos, sin = cos_ref[here, :], sin_ref[here, :]
        for w_ref, dst in ((sq_ref, a_s), (sk_ref, b_s)):
            wide = nn(normed, w_ref[...]).astype(bf).astype(jnp.float32)
            for m in range(2):
                one = wide[:, m * DIFF_HEAD : (m + 1) * DIFF_HEAD]
                turned = one * cos + pltpu.roll(one, DIFF_HEAD // 2, 1) * sin
                dst[here, m * DIFF_HEAD : (m + 1) * DIFF_HEAD] = turned.astype(bf)
        c_s[here, :] = nn(normed, sv_ref[...]).astype(bf)

    levels = CHUNK.bit_length() - 1
    row = lax.broadcasted_iota(jnp.int32, (CHUNK, CHUNK), 0)
    col = lax.broadcasted_iota(jnp.int32, (CHUNK, CHUNK), 1)
    apart = row ^ col

    def advance(first):
        here = pl.ds(first, CHUNK)
        query, key, value = q_s[here, :].astype(jnp.float32), k_s[here, :].astype(jnp.float32), v_s[here, :]
        decay = dec_s[here, :]
        high = decay.astype(bf)
        low = (decay - high.astype(jnp.float32)).astype(bf)
        factors = jnp.exp(nn(span_ref[...], jnp.concatenate([high, low], axis=0)))
        scores = nt(q_s[here, :], k_s[here, :])
        for level in range(levels):
            factor = factors[level * CHUNK : (level + 1) * CHUNK]
            one = nt((query * factor).astype(bf), (key * factor).astype(bf))
            scores = jnp.where((apart >> level) == 1, one, scores)
        scores = jnp.where(row >= col, scores, 0.0).astype(bf)
        gone = factors[levels * CHUNK : (levels + 1) * CHUNK]
        left = factors[(levels + 1) * CHUNK :]
        state = state_s[...]
        raw = nn(scores, value) + nt((query * gone).astype(bf), state.astype(bf))
        state_s[...] = state * gone[CHUNK - 1 :, :] + tn(value, (key * left).astype(bf))
        norm = lax.rsqrt(jnp.mean(raw * raw, axis=-1, keepdims=True) + norm_eps)
        lmix_s[here, :] = (raw * norm * lgain_ref[...]).astype(bf)

    lam = lam_ref[0]
    rate = scale * float(np.log2(np.e))
    key_pos = lax.broadcasted_iota(jnp.int32, (rows, rows), 0)
    query_pos = lax.broadcasted_iota(jnp.int32, (rows, rows), 1)

    def attend_rows(j):
        here = slice(j * rows, (j + 1) * rows)
        spans = [slice(0, j * rows), here] if j else [here]
        pieces = []
        for m in range(2):
            lanes = slice(m * DIFF_HEAD, (m + 1) * DIFF_HEAD)
            scores = [nt(b_s[span, lanes], a_s[here, lanes]) for span in spans]
            scores[-1] = jnp.where(key_pos <= query_pos, scores[-1], -jnp.inf)
            top = functools.reduce(
                jnp.maximum, [jnp.max(one, axis=0, keepdims=True) for one in scores]
            )
            mass = [jnp.exp2((one - top) * rate) for one in scores]
            total = sum(jnp.sum(one, axis=0, keepdims=True) for one in mass)
            mass_ref[j, m : m + 1, :] = top * scale + jnp.log(total)
            pieces.append((mass, 1.0 / total))
        (one, one_rate), (two, two_rate) = pieces
        two_rate = lam * two_rate
        raw = sum(
            tn((u * one_rate - w * two_rate).astype(bf), c_s[span, :])
            for u, w, span in zip(one, two, spans)
        )
        norm = lax.rsqrt(jnp.mean(raw * raw, axis=-1, keepdims=True) + norm_eps)
        smix_s[here, :] = (raw * norm * sgain_ref[...]).astype(bf)

    def leave(p, t):
        here = slice(p * rows, (p + 1) * rows)
        lanes = pl.ds(pl.multiple_of(t * width, width), width)
        full = nn(lmix_s[here, :], lo_ref[:, lanes]) + nn(smix_s[here, :], so_ref[:, lanes])
        part_ref[t, p] = full.astype(bf).reshape(count, piece, width)

    def pair_sum(p):
        landed(pair.at[p], recv1.at[p])
        for i in range(1, count + 1):
            c = lax.rem(me_fs + i, count)
            held[p, c] = (
                part_ref[me_tp, p, c].astype(jnp.float32) + pair[p, c].astype(jnp.float32)
            ).astype(bf)
            if i < count:
                plane_out(p, i).start()

    def plane_sum(p):
        total = held[p, me_fs].astype(jnp.float32)
        for d in range(1, count):
            landed(landing.at[p, d - 1], recv2.at[p, d])
            total = total + landing[p, d - 1].astype(jnp.float32)
        final[p] = total.astype(bf)

        @pl.when(jnp.logical_not(mine(p)))
        def _():
            home_out(p).start()

        @pl.when(mine(p))
        def _():
            pltpu.make_async_copy(final.at[p], out_ref.at[me_fs], recv3.at[me_fs]).start()

    state_s[...] = jnp.zeros_like(state_s)
    arrive(0)
    arrive(1)
    relay(0)
    if planes > 2:
        arrive(2)
    for j in range(planes):
        complete(j)
        if j == 0:
            for load in loads:
                load.wait()
        project_rows(j)
        if j + 3 < planes:
            arrive(j + 3)
        if j + 1 < planes:
            relay(j + 1)
        if j:
            pair_sum(j - 1)
        for n in range(rows // CHUNK):
            advance(j * rows + n * CHUNK)
        attend_rows(j)

        @pl.when(j != me_sp)
        def _():
            mass_out(j).start()

        @pl.when(j == me_sp)
        def _():
            pltpu.make_async_copy(mass_ref.at[j], all_mass_ref.at[j], mrecv.at[j]).start()

        leave(j, other)
        pair_out(j).start()
        leave(j, me_tp)
        if j > 1:
            plane_sum(j - 2)
    pair_sum(planes - 1)
    if planes > 1:
        plane_sum(planes - 2)
    plane_sum(planes - 1)

    for p in range(planes):
        landed(all_mass_ref.at[p], mrecv.at[p])
        pair_out(p).wait_send()
        across(p, 0).wait_send()
        for d in range(1, count):
            spread(p, d).wait_send()
            across(p, d).wait_send()
            plane_out(p, d).wait_send()

        @pl.when(p != me_sp)
        def _():
            mass_out(p).wait_send()

        @pl.when(jnp.logical_not(mine(p)))
        def _():
            home_out(p).wait_send()

    for d in range(1, count):
        rows_out(lax.rem(me_fs + d, count)).wait_send()
    for c in range(count):
        landed(out_ref.at[c], recv3.at[c])

        @pl.when(jnp.logical_not(jnp.logical_and(home, c == me_fs)))
        def _():
            shifts_out(c).wait_send()

        @pl.when(c != me_sp)
        def _():
            rows_on(c).wait_send()


def turned_shards(
    sizes,
    tokens,
    norm_gain,
    lin_query,
    lin_key,
    lin_value,
    lin_decay,
    decay_bias,
    decay_shift,
    soft_query,
    soft_key,
    soft_value,
    soft_lambda,
    lin_gain,
    soft_gain,
    lin_out,
    soft_out,
):
    rows, width = tokens.shape[1:]
    planes, count, parts = sizes["sp"], sizes["fs"], sizes["tp"]
    piece = rows // count
    length = planes * rows
    head = lax.axis_index("fs") * parts + lax.axis_index("tp")
    bf, f32 = jnp.bfloat16, jnp.float32
    vmem = pl.BlockSpec(memory_space=pltpu.VMEM)
    dma = pltpu.SemaphoreType.DMA
    shift = jnp.pad(decay_shift[:, 0, :], ((0, 14), (0, 0)))
    own_lambda = lax.dynamic_slice_in_dim(soft_lambda, head, 1, 0)
    own_bias = lax.dynamic_slice_in_dim(decay_bias, head * GLA_KEY, GLA_KEY, 0)[None]
    cos, sin = turn_tables(length)
    weights = (
        lin_query, lin_key, lin_decay, lin_value, jnp.asarray(cos), jnp.asarray(sin),
        soft_query, soft_key, soft_value, jnp.asarray(level_sums(CHUNK), bf), lin_out, soft_out,
    )
    mixed, all_mass = pl.pallas_call(
        functools.partial(layer_kernel, sizes),
        out_shape=(
            jax.ShapeDtypeStruct((count, piece, width), bf),
            jax.ShapeDtypeStruct((planes, 2, rows), f32),
        ),
        in_specs=[vmem] * 4
        + [pl.BlockSpec(memory_space=pltpu.SMEM)]
        + [vmem] * 2
        + [pl.BlockSpec(memory_space=pl.ANY)] * WEIGHTS,
        out_specs=[vmem] * 2,
        scratch_shapes=[pltpu.VMEM(w.shape, w.dtype) for w in weights]
        + [
            pltpu.VMEM((planes, count, parts, piece, width), bf),
            pltpu.VMEM((planes, 16, rows), bf),
            pltpu.VMEM((length, GLA_KEY), bf),
            pltpu.VMEM((length, GLA_KEY), bf),
            pltpu.VMEM((length, GLA_VALUE), bf),
            pltpu.VMEM((length, GLA_KEY), f32),
            pltpu.VMEM((length, 2 * DIFF_HEAD), bf),
            pltpu.VMEM((length, 2 * DIFF_HEAD), bf),
            pltpu.VMEM((length, DIFF_VALUE), bf),
            pltpu.VMEM((GLA_VALUE, GLA_KEY), f32),
            pltpu.VMEM((length, GLA_VALUE), bf),
            pltpu.VMEM((length, DIFF_VALUE), bf),
            pltpu.VMEM((parts, planes, count, piece, width), bf),
            pltpu.VMEM((planes, 2, rows), f32),
            pltpu.VMEM((planes, count, piece, width), bf),
            pltpu.VMEM((planes, count, piece, width), bf),
            pltpu.VMEM((planes, count - 1, piece, width), bf),
            pltpu.VMEM((planes, piece, width), bf),
            pltpu.VMEM((count, piece, width), bf),
            dma((WEIGHTS,)), dma((count,)), dma((count,)),
            dma((count,)), dma((planes,)), dma((planes, count)), dma((planes, count)),
            dma((planes, count)), dma((planes, count)), dma((count,)), dma((planes,)),
            dma((planes,)), dma((planes,)), dma((planes, count)), dma((planes, count)),
            dma((planes,)), dma((count,)), dma((planes,)), dma((planes,)),
        ],
        compiler_params=pltpu.CompilerParams(
            has_side_effects=True, vmem_limit_bytes=60 * 1024 * 1024
        ),
        name="whole_layer",
    )(
        tokens[0], shift, norm_gain[None], own_bias, own_lambda, lin_gain[None], soft_gain[None],
        *weights,
    )
    return mixed.reshape(1, rows, width), all_mass.transpose(1, 0, 2)[None]


def solution(mesh):
    in_specs = (
        P("fs", "sp", "tp"),
        P(),
        P(None, ("fs", "tp")),
        P(None, ("fs", "tp")),
        P(None, ("fs", "tp")),
        P(None, ("fs", "tp")),
        P(),
        P(None, "fs", "sp"),
        P(None, ("fs", "tp")),
        P(None, ("fs", "tp")),
        P(None, ("fs", "tp")),
        P(),
        P(),
        P(),
        P(("fs", "tp"), None),
        P(("fs", "tp"), None),
    )
    out_specs = (P("fs", "sp", "tp"), P(("fs", "tp"), None, None, "sp"))
    sizes = dict(mesh.shape)

    def per_device(*args):
        one_head = args[2].shape[1] == GLA_KEY and args[10].shape[1] == DIFF_VALUE
        square = sizes["fs"] == sizes["sp"] and sizes["tp"] == 2 and args[0].shape[0] == 1
        if one_head and square:
            return turned_shards(sizes, *args)
        return shards(*args)

    return jax.shard_map(per_device, mesh=mesh, in_specs=in_specs, out_specs=out_specs, check_vma=False)
```

profile of v0, /device:TPU:28, one launch (start us, length us, event | category | flops | bytes accessed | tf_op | source)
XLA Modules:
  0.0 92.1 jit_solution(1366490546152159813)
XLA Ops:
  0.6 0.0 copy-start
  0.7 0.0 copy-start.2
  0.7 0.6 copy-done.2
  1.3 0.6 dynamic_slice.7.lam_ref
  2.0 0.0 copy-done
  2.0 0.6 dynamic-slice_bitcast_fusion.bias_ref
  2.5 0.0 copy-start.1
  2.5 0.7 copy-done.1
  3.2 0.6 pad.4.shift_ref
  3.8 85.1 %whole_layer.1 = (bf16[4,64,1024]{2,1,0:T(8,128)(2,1)}, f32[4,2,256]{2,1,0:T(2,128)}) custom-call(bf16[256,1024]{1,0:T(8,128)(2,1)} %bitcast.11, bf16[16,256]{1,0:T(8,128)(2,1)} %pad.4.shift_ref, f32[1,2048]{1,0:T(1,128)} %bitcast.14, f32[1,128]{1,0:T(1,128)} %dynamic-slice_bitcast_fusion.bias_ref, f32[1]{0:T(128)} %dynamic_slice.7.lam_ref, ...), custom_call_target="tpu_custom_call" | custom-call | tf_op jit(solution)/shard_map/whole_layer/pallas_call | solution.py:767
  89.0 1.3 %copy.21 = f32[1,2,4,256]{3,2,1,0:T(4,128)} copy(f32[1,2,4,256]{3,1,2,0:T(2,128)} %bitcast.13) | data formatting | bytes 16384
  90.3 1.9 %copy.23 = bf16[1,256,1024]{2,1,0:T(8,128)(2,1)} copy(bf16[1,256,1024]{2,1,0:T(8,128)(2,1)} %bitcast.12) | data formatting | bytes 1048576
Async XLA Ops:
  0.6 1.3 %copy-start = (f32[1024]{0:T(1024)S(1)}, f32[1024]{0:T(1024)}, u32[]{:S(2)}) copy-start(f32[1024]{0:T(1024)} %param.25) | copy-start | bytes 12292
  0.7 0.7 copy-start.2
  2.5 0.7 copy-start.1
where the time goes:
time: 92.4 us; the launch traced here: 92.1 us
  Pallas kernels  85.1 us (92%)
  local copies, waits for them, and re-layouts  6.33 us (7%)
    pallas_call x1, Pallas kernels, turned_shards(): pl.pallas_call(functools.partial(layer_kernel, sizes), out_shape=(jax.Sha...  85.1 us
    unnamed x8, local copies, waits for them, and re-layouts  4.5 us

commit v1 on v0

--- a/solution.py
+++ b/solution.py
@@ -396,7 +396,7 @@
     return jnp.dot(a, b, preferred_element_type=jnp.float32)
 
 
-WEIGHTS = 12
+WEIGHTS = 10
 
 
 def layer_kernel(
@@ -404,22 +404,32 @@
     tok_ref, shift_ref, gain_ref, bias_ref, lam_ref, lgain_ref, sgain_ref, *refs,
 ):
     far = refs[:WEIGHTS]
-    out_ref, all_mass_ref = refs[WEIGHTS : WEIGHTS + 2]
-    near = refs[WEIGHTS + 2 : 2 * WEIGHTS + 2]
+    lo_far, so_far = refs[WEIGHTS : WEIGHTS + 2]
+    out_ref, all_mass_ref = refs[WEIGHTS + 2 : WEIGHTS + 4]
+    near = refs[WEIGHTS + 4 : 2 * WEIGHTS + 4]
     (
-        x_ref, rows_ref, q_s, k_s, v_s, dec_s, a_s, b_s, c_s, state_s, lmix_s, smix_s,
-        part_ref, mass_ref, pair, held, landing, final, via,
-        wsem, via_send, via_recv, in_send1, in_recv1, in_send2, in_recv2, in_send3, in_recv3, ssend, srecv,
-        send1, recv1, send2, recv2, send3, recv3, msend, mrecv,
-    ) = refs[2 * WEIGHTS + 2 :]
-    lq_ref, lk_ref, ld_ref, lv_ref, cos_ref, sin_ref, sq_ref, sk_ref, sv_ref, span_ref, lo_ref, so_ref = near
+        wout_ref, x_ref, rows_ref, q_s, k_s, v_s, dec_s, a_s, b_s, c_s, state_s, mix_s, omix_s,
+        mass_ref, via, via_shift, own_s, later_s, first_x, first_y, got_x, got_y,
+        second_x, second_y, more_x, more_y, final,
+        wsem, osem, wo_send, wo_recv, sc_send, via_recv, z_send, in_recv,
+        sh_send, sh_recv, shz_send, shz_recv,
+        g_send, g_recv, h_send, h_recv, ac_send, ac_recv, mix_send, mix_recv,
+        f_send, f_recv, s_send, s_recv, home_send, home_recv, msend, mrecv,
+    ) = refs[2 * WEIGHTS + 4 :]
+    lq_ref, lk_ref, ld_ref, lv_ref, cos_ref, sin_ref, sq_ref, sk_ref, sv_ref, span_ref = near
     planes, count, parts, piece, width = x_ref.shape
     rows = count * piece
+    half = piece // 2
     scale = DIFF_HEAD ** (-0.5)
     bf = jnp.bfloat16
     me_sp, me_fs, me_tp = lax.axis_index("sp"), lax.axis_index("fs"), lax.axis_index("tp")
     other = 1 - me_tp
     home = me_sp == me_fs
+    low, high_bit = me_fs % 2, me_fs // 2
+    beside = high_bit * 2 + 1 - low
+    above = (1 - high_bit) * 2 + low
+    across_from = (1 - high_bit) * 2 + 1 - low
+    columns = (me_fs, beside, above, across_from)
 
     def remote(src, dst, send, recv, sp, fs, tp):
         return pltpu.make_async_remote_copy(
@@ -434,51 +444,89 @@
     def landed(ref, sem):
         pltpu.make_async_copy(ref, ref, sem).wait()
 
-    def rows_out(c):
-        return remote(
-            tok_ref.at[pl.ds(c * piece, piece)], via.at[me_fs],
-            via_send.at[c], via_recv.at[me_fs], me_sp, c, me_tp,
-        )
-
-    def rows_on(z):
-        return remote(
-            via.at[z], x_ref.at[me_sp, me_fs, me_tp],
-            in_send1.at[z], in_recv1.at[me_sp], z, me_fs, me_tp,
-        )
-
-    def shifts_out(c):
-        return remote(
-            shift_ref, rows_ref.at[me_sp], ssend.at[c], srecv.at[me_sp], me_fs, c, me_tp
-        )
-
-    def spread(p, d):
+    def piece_of(c):
+        return tok_ref.at[pl.ds(pl.multiple_of(c * piece, piece), piece)]
+
+    def rows_out(r):
+        c = columns[r]
+        return remote(
+            piece_of(c), via.at[r - 1], sc_send.at[r - 1], via_recv.at[r - 1], me_sp, c, me_tp
+        )
+
+    def rows_home(r):
+        c = columns[r]
+        return remote(
+            piece_of(c), x_ref.at[me_sp, c, me_tp],
+            sc_send.at[r - 1], in_recv.at[me_sp], me_sp, c, me_tp,
+        )
+
+    def rows_on(r):
+        src = piece_of(me_fs) if r == 0 else via.at[r - 1]
+        return remote(
+            src, x_ref.at[me_sp, me_fs, me_tp],
+            z_send.at[r], in_recv.at[me_sp], columns[r], me_fs, me_tp,
+        )
+
+    def shift_out(r):
+        return remote(
+            shift_ref, via_shift.at[r - 1],
+            sh_send.at[r - 1], sh_recv.at[r - 1], me_sp, columns[r], me_tp,
+        )
+
+    def shift_on(r):
+        src = shift_ref if r == 0 else via_shift.at[r - 1]
+        return remote(
+            src, rows_ref.at[me_sp], shz_send.at[r], shz_recv.at[me_sp], columns[r], me_fs, me_tp
+        )
+
+    def near_copy(p, r):
         block = x_ref.at[p, me_fs, me_tp]
         return remote(
-            block, block, in_send2.at[p, d], in_recv2.at[p, d],
-            me_sp, lax.rem(me_fs + d, count), me_tp,
-        )
-
-    def source(d):
-        return lax.rem(me_fs + count - d, count)
-
-    def across(p, d):
-        block = x_ref.at[p, source(d), me_tp]
-        return remote(block, block, in_send3.at[p, d], in_recv3.at[p, d], me_sp, me_fs, other)
-
-    def pair_out(p):
-        return remote(
-            part_ref.at[other, p], pair.at[p], send1.at[p], recv1.at[p], me_sp, me_fs, other
-        )
-
-    def plane_out(p, d):
-        c = lax.rem(me_fs + d, count)
-        return remote(
-            held.at[p, c], landing.at[p, d - 1], send2.at[p, d], recv2.at[p, d], me_sp, c, me_tp
+            block, block, g_send.at[p, r - 1], g_recv.at[p, r - 1], me_sp, columns[r], me_tp
+        )
+
+    def half_copy(p, r):
+        block = x_ref.at[p, columns[3 - r], me_tp, pl.ds((r % 2) * half, half)]
+        return remote(
+            block, block, h_send.at[p, r - 1], h_recv.at[p, r - 1], me_sp, columns[r], me_tp
+        )
+
+    def across(p, r):
+        if r < 3:
+            block = x_ref.at[p, columns[r], me_tp]
+        else:
+            block = x_ref.at[p, columns[3], me_tp, pl.ds((r - 3) * half, half)]
+        return remote(block, block, ac_send.at[p, r], ac_recv.at[p, r], me_sp, me_fs, other)
+
+    def crossed(p, r):
+        if r < 3:
+            landed(x_ref.at[p, columns[r], other], ac_recv.at[p, r])
+        else:
+            landed(x_ref.at[p, columns[3], other, pl.ds((r - 3) * half, half)], ac_recv.at[p, r])
+
+    def mix_out(j):
+        here = pl.ds(j * rows, rows)
+        return remote(
+            mix_s.at[here], omix_s.at[here], mix_send.at[j], mix_recv.at[j], me_sp, me_fs, other
+        )
+
+    def first_out(j, r):
+        src, dst = (first_x, got_x) if r == 1 else (first_y, got_y)
+        return remote(
+            src.at[j], dst.at[j], f_send.at[j, r - 1], f_recv.at[j, r - 1],
+            me_sp, columns[r], me_tp,
+        )
+
+    def second_out(j, r):
+        src, dst = (second_x, more_x) if r == 1 else (second_y, more_y)
+        return remote(
+            src.at[j], dst.at[j], s_send.at[j, r - 1], s_recv.at[j, r - 1],
+            me_sp, columns[r], me_tp,
         )
 
     def home_out(p):
         return remote(
-            final.at[p], out_ref.at[me_fs], send3.at[p], recv3.at[me_fs], p, me_sp, me_tp
+            final.at[p], out_ref.at[me_fs], home_send.at[p], home_recv.at[me_fs], p, me_sp, me_tp
         )
 
     def mass_out(p):
@@ -489,59 +537,106 @@
     def mine(p):
         return jnp.logical_and(home, p == me_sp)
 
+    def own_cols(t):
+        return pl.ds(pl.multiple_of(t * width, width), width)
+
     loads = [pltpu.make_async_copy(f, n, wsem.at[i]) for i, (f, n) in enumerate(zip(far, near))]
-
-    for d in range(1, count):
-        rows_out(lax.rem(me_fs + d, count)).start()
-    pltpu.make_async_copy(
-        tok_ref.at[pl.ds(me_fs * piece, piece)], via.at[me_fs], via_recv.at[me_fs]
-    ).start()
-    for c in range(count):
-        own = jnp.logical_and(home, c == me_fs)
-
-        @pl.when(jnp.logical_not(own))
-        def _():
-            shifts_out(c).start()
-
-        @pl.when(own)
-        def _():
-            pltpu.make_async_copy(shift_ref, rows_ref.at[me_sp], srecv.at[me_sp]).start()
-
-    for d in range(count):
-        z = lax.rem(me_fs + d, count)
-        landed(via.at[z], via_recv.at[z])
-
-        @pl.when(z != me_sp)
-        def _():
-            rows_on(z).start()
-
-        @pl.when(z == me_sp)
-        def _():
-            pltpu.make_async_copy(
-                via.at[z], x_ref.at[me_sp, me_fs, me_tp], in_recv1.at[me_sp]
-            ).start()
-
+    depth = lo_far.shape[0]
+    out_loads = [
+        pltpu.make_async_copy(
+            f.at[:, own_cols(me_tp)], wout_ref.at[0, pl.ds(i * depth, depth)], osem.at[i]
+        )
+        for i, f in enumerate((lo_far, so_far))
+    ]
+    out_gives = [
+        remote(
+            f.at[:, own_cols(other)], wout_ref.at[1, pl.ds(i * depth, depth)],
+            wo_send.at[i], wo_recv.at[i], me_sp, me_fs, other,
+        )
+        for i, f in enumerate((lo_far, so_far))
+    ]
+
+    barrier = pltpu.get_barrier_semaphore()
+    partners = [(me_sp, c, me_tp) for c in columns[1:]] + [(me_sp, me_fs, other)]
+    partners += [(lax.rem(me_sp + d, planes), me_fs, me_tp) for d in range(1, planes)]
+    for sp, fs, tp in partners:
+        pl.semaphore_signal(
+            barrier, inc=1, device_id={"sp": sp, "fs": fs, "tp": tp},
+            device_id_type=pl.DeviceIdType.MESH,
+        )
     for load in loads:
         load.start()
+    for load in out_loads:
+        load.start()
+    pl.semaphore_wait(barrier, len(partners))
+
+    @pl.when(home)
+    def _():
+        for r in (3, 1, 2):
+            rows_home(r).start()
+        pltpu.make_async_copy(
+            piece_of(me_fs), x_ref.at[me_sp, me_fs, me_tp], in_recv.at[me_sp]
+        ).start()
+        pltpu.make_async_copy(shift_ref, rows_ref.at[me_sp], shz_recv.at[me_sp]).start()
+
+    @pl.when(jnp.logical_not(home))
+    def _():
+        for r in (3, 1, 2):
+            rows_out(r).start()
+        rows_on(0).start()
+        shift_on(0).start()
+
+    for r in (1, 2, 3):
+        shift_out(r).start()
+
+    def forward(r):
+        stay = columns[r] == me_sp
+
+        @pl.when(jnp.logical_not(stay))
+        def _():
+            landed(via.at[r - 1], via_recv.at[r - 1])
+            rows_on(r).start()
+            landed(via_shift.at[r - 1], sh_recv.at[r - 1])
+            shift_on(r).start()
+
+        @pl.when(stay)
+        def _():
+            landed(via_shift.at[r - 1], sh_recv.at[r - 1])
+            pltpu.make_async_copy(
+                via_shift.at[r - 1], rows_ref.at[me_sp], shz_recv.at[me_sp]
+            ).start()
+
+    for r in (1, 2, 3):
+        forward(r)
+    for give in out_gives:
+        give.start()
 
     def arrive(p):
-        landed(x_ref.at[p, me_fs, me_tp], in_recv1.at[p])
-        for d in range(1, count):
-            spread(p, d).start()
+        landed(x_ref.at[p, me_fs, me_tp], in_recv.at[p])
+        near_copy(p, 1).start()
+        near_copy(p, 2).start()
         across(p, 0).start()
 
     def relay(p):
-        for d in range(1, count):
-            landed(x_ref.at[p, source(d), me_tp], in_recv2.at[p, d])
-            across(p, d).start()
+        for r in (1, 2):
+            landed(x_ref.at[p, columns[r], me_tp], g_recv.at[p, r - 1])
+            half_copy(p, 3 - r).start()
+            across(p, r).start()
+
+    def gather_rest(p):
+        for r in (1, 2):
+            landed(
+                x_ref.at[p, columns[3], me_tp, pl.ds((r % 2) * half, half)], h_recv.at[p, r - 1]
+            )
+            across(p, 3 + r % 2).start()
 
     def complete(p):
-        for d in range(count):
-            landed(x_ref.at[p, source(d), other], in_recv3.at[p, d])
-        landed(rows_ref.at[p], srecv.at[p])
+        for r in range(5):
+            crossed(p, r)
+        landed(rows_ref.at[p], shz_recv.at[p])
 
     def project_rows(p):
-        here = pl.ds(p * rows, rows)
+        here = pl.ds(pl.multiple_of(p * rows, rows), rows)
         halves = [x_ref[p, :, t].reshape(rows, width).astype(jnp.float32) for t in range(parts)]
         square = sum(jnp.sum(h * h, axis=-1, keepdims=True) for h in halves)
         factor = lax.rsqrt(square / (parts * width) + norm_eps)
@@ -596,7 +691,7 @@
         raw = nn(scores, value) + nt((query * gone).astype(bf), state.astype(bf))
         state_s[...] = state * gone[CHUNK - 1 :, :] + tn(value, (key * left).astype(bf))
         norm = lax.rsqrt(jnp.mean(raw * raw, axis=-1, keepdims=True) + norm_eps)
-        lmix_s[here, :] = (raw * norm * lgain_ref[...]).astype(bf)
+        mix_s[here, :GLA_VALUE] = (raw * norm * lgain_ref[...]).astype(bf)
 
     lam = lam_ref[0]
     rate = scale * float(np.log2(np.e))
@@ -625,87 +720,136 @@
             for u, w, span in zip(one, two, spans)
         )
         norm = lax.rsqrt(jnp.mean(raw * raw, axis=-1, keepdims=True) + norm_eps)
-        smix_s[here, :] = (raw * norm * sgain_ref[...]).astype(bf)
-
-    def leave(p, t):
-        here = slice(p * rows, (p + 1) * rows)
-        lanes = pl.ds(pl.multiple_of(t * width, width), width)
-        full = nn(lmix_s[here, :], lo_ref[:, lanes]) + nn(smix_s[here, :], so_ref[:, lanes])
-        part_ref[t, p] = full.astype(bf).reshape(count, piece, width)
-
-    def pair_sum(p):
-        landed(pair.at[p], recv1.at[p])
-        for i in range(1, count + 1):
-            c = lax.rem(me_fs + i, count)
-            held[p, c] = (
-                part_ref[me_tp, p, c].astype(jnp.float32) + pair[p, c].astype(jnp.float32)
-            ).astype(bf)
-            if i < count:
-                plane_out(p, i).start()
-
-    def plane_sum(p):
-        total = held[p, me_fs].astype(jnp.float32)
-        for d in range(1, count):
-            landed(landing.at[p, d - 1], recv2.at[p, d])
-            total = total + landing[p, d - 1].astype(jnp.float32)
-        final[p] = total.astype(bf)
-
-        @pl.when(jnp.logical_not(mine(p)))
+        mix_s[here, GLA_VALUE:] = (raw * norm * sgain_ref[...]).astype(bf)
+
+        @pl.when(j != me_sp)
         def _():
-            home_out(p).start()
-
-        @pl.when(mine(p))
+            mass_out(j).start()
+
+        @pl.when(j == me_sp)
         def _():
-            pltpu.make_async_copy(final.at[p], out_ref.at[me_fs], recv3.at[me_fs]).start()
-
-    state_s[...] = jnp.zeros_like(state_s)
-    arrive(0)
-    arrive(1)
-    relay(0)
-    if planes > 2:
-        arrive(2)
-    for j in range(planes):
-        complete(j)
-        if j == 0:
-            for load in loads:
-                load.wait()
-        project_rows(j)
-        if j + 3 < planes:
-            arrive(j + 3)
-        if j + 1 < planes:
-            relay(j + 1)
-        if j:
-            pair_sum(j - 1)
+            pltpu.make_async_copy(mass_ref.at[j], all_mass_ref.at[j], mrecv.at[j]).start()
+
+    def mix_rows(j):
         for n in range(rows // CHUNK):
             advance(j * rows + n * CHUNK)
         attend_rows(j)
-
-        @pl.when(j != me_sp)
+        mix_out(j).start()
+
+    def leave(j):
+        landed(omix_s.at[pl.ds(j * rows, rows)], mix_recv.at[j])
+
+        def turned(ref):
+            return jnp.concatenate(
+                [
+                    ref[pl.ds(pl.multiple_of(j * rows + c * piece, piece), piece), :]
+                    for c in columns
+                ],
+                axis=0,
+            )
+
+        full = nn(turned(mix_s), wout_ref[0]) + nn(turned(omix_s), wout_ref[1])
+        parted = [full[i * half : (i + 1) * half] for i in range(2 * count)]
+        first_x[j, 0] = parted[2].astype(bf)
+        first_x[j, 1] = parted[6].astype(bf)
+        first_y[j, 0] = parted[5].astype(bf)
+        first_y[j, 1] = parted[7].astype(bf)
+        own_s[j, 0] = parted[0]
+        own_s[j, 1] = parted[1]
+        later_s[j, 0] = parted[3]
+        later_s[j, 1] = parted[4]
+        first_out(j, 1).start()
+        first_out(j, 2).start()
+
+    def pass_on(j):
+        landed(got_x.at[j], f_recv.at[j, 0])
+        second_y[j] = (later_s[j, 1] + got_x[j, 1].astype(jnp.float32)).astype(bf)
+        second_out(j, 2).start()
+        landed(got_y.at[j], f_recv.at[j, 1])
+        second_x[j] = (later_s[j, 0] + got_y[j, 1].astype(jnp.float32)).astype(bf)
+        second_out(j, 1).start()
+
+    def finish(j):
+        landed(more_y.at[j], s_recv.at[j, 1])
+        final[j, pl.ds(0, half)] = (
+            own_s[j, 0] + got_x[j, 0].astype(jnp.float32) + more_y[j].astype(jnp.float32)
+        ).astype(bf)
+        landed(more_x.at[j], s_recv.at[j, 0])
+        final[j, pl.ds(half, half)] = (
+            own_s[j, 1] + got_y[j, 0].astype(jnp.float32) + more_x[j].astype(jnp.float32)
+        ).astype(bf)
+
+        @pl.when(jnp.logical_not(mine(j)))
         def _():
-            mass_out(j).start()
-
-        @pl.when(j == me_sp)
+            home_out(j).start()
+
+        @pl.when(mine(j))
         def _():
-            pltpu.make_async_copy(mass_ref.at[j], all_mass_ref.at[j], mrecv.at[j]).start()
-
-        leave(j, other)
-        pair_out(j).start()
-        leave(j, me_tp)
-        if j > 1:
-            plane_sum(j - 2)
-    pair_sum(planes - 1)
-    if planes > 1:
-        plane_sum(planes - 2)
-    plane_sum(planes - 1)
+            pltpu.make_async_copy(final.at[j], out_ref.at[me_fs], home_recv.at[me_fs]).start()
+
+    def slot(i):
+        if i == 0:
+            return me_sp
+        return i - 1 + (i - 1 >= me_sp).astype(jnp.int32)
+
+    state_s[...] = jnp.zeros_like(state_s)
+    order = [slot(i) for i in range(planes)]
+    arrive(order[0])
+    relay(order[0])
+    arrive(order[1])
+    gather_rest(order[0])
+    complete(order[0])
+    for load in loads:
+        load.wait()
+    project_rows(order[0])
+
+    relay(order[1])
+    arrive(order[2])
+    gather_rest(order[1])
+    complete(order[1])
+    project_rows(order[1])
+    mix_rows(0)
+
+    relay(order[2])
+    arrive(order[3])
+    for load in out_loads:
+        load.wait()
+    for give in out_gives:
+        give.wait_recv()
+    leave(0)
+    gather_rest(order[2])
+    complete(order[2])
+    project_rows(order[2])
+    mix_rows(1)
+
+    relay(order[3])
+    leave(1)
+    pass_on(0)
+    gather_rest(order[3])
+    complete(order[3])
+    project_rows(order[3])
+    mix_rows(2)
+    finish(0)
+    pass_on(1)
+    leave(2)
+    mix_rows(3)
+    finish(1)
+    pass_on(2)
+    leave(3)
+    finish(2)
+    pass_on(3)
+    finish(3)
 
     for p in range(planes):
         landed(all_mass_ref.at[p], mrecv.at[p])
-        pair_out(p).wait_send()
-        across(p, 0).wait_send()
-        for d in range(1, count):
-            spread(p, d).wait_send()
-            across(p, d).wait_send()
-            plane_out(p, d).wait_send()
+        mix_out(p).wait_send()
+        for r in range(5):
+            across(p, r).wait_send()
+        for r in (1, 2):
+            near_copy(p, r).wait_send()
+            half_copy(p, r).wait_send()
+            first_out(p, r).wait_send()
+            second_out(p, r).wait_send()
 
         @pl.when(p != me_sp)
         def _():
@@ -715,18 +859,25 @@
         def _():
             home_out(p).wait_send()
 
-    for d in range(1, count):
-        rows_out(lax.rem(me_fs + d, count)).wait_send()
+    for give in out_gives:
+        give.wait_send()
+
+    @pl.when(jnp.logical_not(home))
+    def _():
+        rows_on(0).wait_send()
+        shift_on(0).wait_send()
+
+    for r in (1, 2, 3):
+        rows_out(r).wait_send()
+        shift_out(r).wait_send()
+
+        @pl.when(columns[r] != me_sp)
+        def _():
+            rows_on(r).wait_send()
+            shift_on(r).wait_send()
+
     for c in range(count):
-        landed(out_ref.at[c], recv3.at[c])
-
-        @pl.when(jnp.logical_not(jnp.logical_and(home, c == me_fs)))
-        def _():
-            shifts_out(c).wait_send()
-
-        @pl.when(c != me_sp)
-        def _():
-            rows_on(c).wait_send()
+        landed(out_ref.at[c], home_recv.at[c])
 
 
 def turned_shards(
@@ -751,6 +902,7 @@
     rows, width = tokens.shape[1:]
     planes, count, parts = sizes["sp"], sizes["fs"], sizes["tp"]
     piece = rows // count
+    half = piece // 2
     length = planes * rows
     head = lax.axis_index("fs") * parts + lax.axis_index("tp")
     bf, f32 = jnp.bfloat16, jnp.float32
@@ -762,7 +914,7 @@
     cos, sin = turn_tables(length)
     weights = (
         lin_query, lin_key, lin_decay, lin_value, jnp.asarray(cos), jnp.asarray(sin),
-        soft_query, soft_key, soft_value, jnp.asarray(level_sums(CHUNK), bf), lin_out, soft_out,
+        soft_query, soft_key, soft_value, jnp.asarray(level_sums(CHUNK), bf),
     )
     mixed, all_mass = pl.pallas_call(
         functools.partial(layer_kernel, sizes),
@@ -773,10 +925,11 @@
         in_specs=[vmem] * 4
         + [pl.BlockSpec(memory_space=pltpu.SMEM)]
         + [vmem] * 2
-        + [pl.BlockSpec(memory_space=pl.ANY)] * WEIGHTS,
+        + [pl.BlockSpec(memory_space=pl.ANY)] * (WEIGHTS + 2),
         out_specs=[vmem] * 2,
         scratch_shapes=[pltpu.VMEM(w.shape, w.dtype) for w in weights]
         + [
+            pltpu.VMEM((2, GLA_VALUE + DIFF_VALUE, width), bf),
             pltpu.VMEM((planes, count, parts, piece, width), bf),
             pltpu.VMEM((planes, 16, rows), bf),
             pltpu.VMEM((length, GLA_KEY), bf),
@@ -787,28 +940,37 @@
             pltpu.VMEM((length, 2 * DIFF_HEAD), bf),
             pltpu.VMEM((length, DIFF_VALUE), bf),
             pltpu.VMEM((GLA_VALUE, GLA_KEY), f32),
-            pltpu.VMEM((length, GLA_VALUE), bf),
-            pltpu.VMEM((length, DIFF_VALUE), bf),
-            pltpu.VMEM((parts, planes, count, piece, width), bf),
+            pltpu.VMEM((length, GLA_VALUE + DIFF_VALUE), bf),
+            pltpu.VMEM((length, GLA_VALUE + DIFF_VALUE), bf),
             pltpu.VMEM((planes, 2, rows), f32),
-            pltpu.VMEM((planes, count, piece, width), bf),
-            pltpu.VMEM((planes, count, piece, width), bf),
-            pltpu.VMEM((planes, count - 1, piece, width), bf),
+            pltpu.VMEM((count - 1, piece, width), bf),
+            pltpu.VMEM((count - 1, 16, rows), bf),
+            pltpu.VMEM((planes, 2, half, width), f32),
+            pltpu.VMEM((planes, 2, half, width), f32),
+            pltpu.VMEM((planes, 2, half, width), bf),
+            pltpu.VMEM((planes, 2, half, width), bf),
+            pltpu.VMEM((planes, 2, half, width), bf),
+            pltpu.VMEM((planes, 2, half, width), bf),
+            pltpu.VMEM((planes, half, width), bf),
+            pltpu.VMEM((planes, half, width), bf),
+            pltpu.VMEM((planes, half, width), bf),
+            pltpu.VMEM((planes, half, width), bf),
             pltpu.VMEM((planes, piece, width), bf),
-            pltpu.VMEM((count, piece, width), bf),
-            dma((WEIGHTS,)), dma((count,)), dma((count,)),
-            dma((count,)), dma((planes,)), dma((planes, count)), dma((planes, count)),
-            dma((planes, count)), dma((planes, count)), dma((count,)), dma((planes,)),
-            dma((planes,)), dma((planes,)), dma((planes, count)), dma((planes, count)),
+            dma((WEIGHTS,)), dma((2,)), dma((2,)), dma((2,)),
+            dma((count - 1,)), dma((count - 1,)), dma((count,)), dma((planes,)),
+            dma((count - 1,)), dma((count - 1,)), dma((count,)), dma((planes,)),
+            dma((planes, 2)), dma((planes, 2)), dma((planes, 2)), dma((planes, 2)),
+            dma((planes, 5)), dma((planes, 5)), dma((planes,)), dma((planes,)),
+            dma((planes, 2)), dma((planes, 2)), dma((planes, 2)), dma((planes, 2)),
             dma((planes,)), dma((count,)), dma((planes,)), dma((planes,)),
         ],
         compiler_params=pltpu.CompilerParams(
-            has_side_effects=True, vmem_limit_bytes=60 * 1024 * 1024
+            has_side_effects=True, collective_id=0, vmem_limit_bytes=60 * 1024 * 1024
         ),
         name="whole_layer",
     )(
         tokens[0], shift, norm_gain[None], own_bias, own_lambda, lin_gain[None], soft_gain[None],
-        *weights,
+        *weights, lin_out, soft_out,
     )
     return mixed.reshape(1, rows, width), all_mass.transpose(1, 0, 2)[None]
 
@@ -837,7 +999,7 @@
 
     def per_device(*args):
         one_head = args[2].shape[1] == GLA_KEY and args[10].shape[1] == DIFF_VALUE
-        square = sizes["fs"] == sizes["sp"] and sizes["tp"] == 2 and args[0].shape[0] == 1
+        square = sizes["fs"] == sizes["sp"] == 4 and sizes["tp"] == 2 and args[0].shape[0] == 1
         if one_head and square:
             return turned_shards(sizes, *args)
         return shards(*args)

time: 92.4 us -> 89.6 us (0.970)
  the two profiles are of different devices: /device:TPU:28 before, /device:TPU:26 now
where the time goes in v1:
time: 89.6 us; the launch traced here: 89.3 us
  Pallas kernels  82.3 us (92%)
  local copies, waits for them, and re-layouts  6.33 us (7%)
    pallas_call x1, Pallas kernels, turned_shards(): pl.pallas_call(functools.partial(layer_kernel, sizes), out_shape=(jax.Sha...  82.3 us
    unnamed x8, local copies, waits for them, and re-layouts  4.5 us

profile of v1, /device:TPU:26, one launch (start us, length us, event | category | flops | bytes accessed | tf_op | source)
XLA Modules:
  0.0 89.3 jit_solution(1860512080783755790)
XLA Ops:
  0.6 0.0 copy-start
  0.7 0.0 copy-start.2
  0.7 0.6 copy-done.2
  1.3 0.6 dynamic_slice.7.lam_ref
  2.0 0.0 copy-done
  2.0 0.6 dynamic-slice_bitcast_fusion.bias_ref
  2.5 0.0 copy-start.1
  2.5 0.7 copy-done.1
  3.2 0.6 pad.4.shift_ref
  3.8 82.3 %whole_layer.1 = (bf16[4,64,1024]{2,1,0:T(8,128)(2,1)}, f32[4,2,256]{2,1,0:T(2,128)}) custom-call(bf16[256,1024]{1,0:T(8,128)(2,1)} %bitcast.11, bf16[16,256]{1,0:T(8,128)(2,1)} %pad.4.shift_ref, f32[1,2048]{1,0:T(1,128)} %bitcast.14, f32[1,128]{1,0:T(1,128)} %dynamic-slice_bitcast_fusion.bias_ref, f32[1]{0:T(128)} %dynamic_slice.7.lam_ref, ...), custom_call_target="tpu_custom_call" | custom-call | tf_op jit(solution)/shard_map/whole_layer/pallas_call | solution.py:919
  86.1 1.3 %copy.21 = f32[1,2,4,256]{3,2,1,0:T(4,128)} copy(f32[1,2,4,256]{3,1,2,0:T(2,128)} %bitcast.13) | data formatting | bytes 16384
  87.4 1.9 %copy.23 = bf16[1,256,1024]{2,1,0:T(8,128)(2,1)} copy(bf16[1,256,1024]{2,1,0:T(8,128)(2,1)} %bitcast.12) | data formatting | bytes 1048576
Async XLA Ops:
  0.6 1.3 %copy-start = (f32[1024]{0:T(1024)S(1)}, f32[1024]{0:T(1024)}, u32[]{:S(2)}) copy-start(f32[1024]{0:T(1024)} %param.25) | copy-start | bytes 12292
  0.7 0.7 copy-start.2
  2.5 0.7 copy-start.1

commit v2 on v1

--- a/solution.py
+++ b/solution.py
@@ -396,30 +396,33 @@
     return jnp.dot(a, b, preferred_element_type=jnp.float32)
 
 
-WEIGHTS = 10
+WEIGHTS = 17
 
 
 def layer_kernel(
     sizes,
-    tok_ref, shift_ref, gain_ref, bias_ref, lam_ref, lgain_ref, sgain_ref, *refs,
+    *refs,
 ):
     far = refs[:WEIGHTS]
     lo_far, so_far = refs[WEIGHTS : WEIGHTS + 2]
     out_ref, all_mass_ref = refs[WEIGHTS + 2 : WEIGHTS + 4]
     near = refs[WEIGHTS + 4 : 2 * WEIGHTS + 4]
     (
-        wout_ref, x_ref, rows_ref, q_s, k_s, v_s, dec_s, a_s, b_s, c_s, state_s, mix_s, omix_s,
-        mass_ref, via, via_shift, own_s, later_s, first_x, first_y, got_x, got_y,
+        wout_ref, x_ref, rows_ref, normed_s, q_s, k_s, v_s, dec_s, a_s, b_s, c_s, state_s, mix_s, omix_s,
+        mass_ref, mass_in, via, via_shift, own_s, later_s, first_x, first_y, got_x, got_y,
         second_x, second_y, more_x, more_y, final,
         wsem, osem, wo_send, wo_recv, sc_send, via_recv, z_send, in_recv,
         sh_send, sh_recv, shz_send, shz_recv,
         g_send, g_recv, h_send, h_recv, ac_send, ac_recv, mix_send, mix_recv,
         f_send, f_recv, s_send, s_recv, home_send, home_recv, msend, mrecv,
     ) = refs[2 * WEIGHTS + 4 :]
-    lq_ref, lk_ref, ld_ref, lv_ref, cos_ref, sin_ref, sq_ref, sk_ref, sv_ref, span_ref = near
+    (
+        tok_ref, shift_ref, gain_ref, bias_ref, lam_ref, lgain_ref, sgain_ref,
+        lq_ref, lk_ref, ld_ref, lv_ref, cos_ref, sin_ref, sq_ref, sk_ref, sv_ref, span_ref,
+    ) = near
     planes, count, parts, piece, width = x_ref.shape
     rows = count * piece
-    half = piece // 2
+    half, quarter = piece // 2, piece // 4
     scale = DIFF_HEAD ** (-0.5)
     bf = jnp.bfloat16
     me_sp, me_fs, me_tp = lax.axis_index("sp"), lax.axis_index("fs"), lax.axis_index("tp")
@@ -444,27 +447,27 @@
     def landed(ref, sem):
         pltpu.make_async_copy(ref, ref, sem).wait()
 
-    def piece_of(c):
-        return tok_ref.at[pl.ds(pl.multiple_of(c * piece, piece), piece)]
-
-    def rows_out(r):
+    def piece_of(c, h=0, count_of=2):
+        return tok_ref.at[pl.ds(pl.multiple_of(c * piece + h * half, half), count_of * half)]
+
+    def rows_out(r, h):
+        return remote(
+            piece_of(columns[r], h, 1), via.at[r - 1, h],
+            sc_send.at[r - 1, h], via_recv.at[r - 1, h], me_sp, columns[r], me_tp,
+        )
+
+    def rows_home(r, h):
         c = columns[r]
         return remote(
-            piece_of(c), via.at[r - 1], sc_send.at[r - 1], via_recv.at[r - 1], me_sp, c, me_tp
-        )
-
-    def rows_home(r):
-        c = columns[r]
+            piece_of(c, h, 1), x_ref.at[me_sp, c, me_tp, pl.ds(h * half, half)],
+            sc_send.at[r - 1, h], in_recv.at[me_sp, h], me_sp, c, me_tp,
+        )
+
+    def rows_on(r, h):
+        src = piece_of(me_fs, h, 1) if r == 0 else via.at[r - 1, h]
         return remote(
-            piece_of(c), x_ref.at[me_sp, c, me_tp],
-            sc_send.at[r - 1], in_recv.at[me_sp], me_sp, c, me_tp,
-        )
-
-    def rows_on(r):
-        src = piece_of(me_fs) if r == 0 else via.at[r - 1]
-        return remote(
-            src, x_ref.at[me_sp, me_fs, me_tp],
-            z_send.at[r], in_recv.at[me_sp], columns[r], me_fs, me_tp,
+            src, x_ref.at[me_sp, me_fs, me_tp, pl.ds(h * half, half)],
+            z_send.at[r, h], in_recv.at[me_sp, h], columns[r], me_fs, me_tp,
         )
 
     def shift_out(r):
@@ -479,10 +482,14 @@
             src, rows_ref.at[me_sp], shz_send.at[r], shz_recv.at[me_sp], columns[r], me_fs, me_tp
         )
 
-    def near_copy(p, r):
-        block = x_ref.at[p, me_fs, me_tp]
+    def half_of(p, c, h):
+        return x_ref.at[p, c, me_tp, pl.ds(h * half, half)]
+
+    def near_copy(p, r, k):
+        block = half_of(p, me_fs, (r - 1 + k) % 2)
         return remote(
-            block, block, g_send.at[p, r - 1], g_recv.at[p, r - 1], me_sp, columns[r], me_tp
+            block, block, g_send.at[p, r - 1, k], g_recv.at[p, r - 1, k],
+            me_sp, columns[r], me_tp,
         )
 
     def half_copy(p, r):
@@ -504,34 +511,44 @@
         else:
             landed(x_ref.at[p, columns[3], other, pl.ds((r - 3) * half, half)], ac_recv.at[p, r])
 
+    def block_rows(j):
+        return pl.ds(pl.multiple_of(j * rows, rows), rows)
+
     def mix_out(j):
-        here = pl.ds(j * rows, rows)
+        here = block_rows(j)
         return remote(
             mix_s.at[here], omix_s.at[here], mix_send.at[j], mix_recv.at[j], me_sp, me_fs, other
         )
 
-    def first_out(j, r):
+    def first_out(j, u, r):
         src, dst = (first_x, got_x) if r == 1 else (first_y, got_y)
         return remote(
-            src.at[j], dst.at[j], f_send.at[j, r - 1], f_recv.at[j, r - 1],
+            src.at[j, u], dst.at[j, u], f_send.at[j, u, r - 1], f_recv.at[j, u, r - 1],
             me_sp, columns[r], me_tp,
         )
 
-    def second_out(j, r):
+    def second_out(j, u, r):
         src, dst = (second_x, more_x) if r == 1 else (second_y, more_y)
         return remote(
-            src.at[j], dst.at[j], s_send.at[j, r - 1], s_recv.at[j, r - 1],
+            src.at[j, u], dst.at[j, u], s_send.at[j, u, r - 1], s_recv.at[j, u, r - 1],
             me_sp, columns[r], me_tp,
         )
 
-    def home_out(p):
+    def final_rows(p, u):
+        return final.at[p, pl.ds(u * half, half)]
+
+    def out_rows(c, u):
+        return out_ref.at[c, pl.ds(u * half, half)]
+
+    def home_out(p, u):
         return remote(
-            final.at[p], out_ref.at[me_fs], home_send.at[p], home_recv.at[me_fs], p, me_sp, me_tp
+            final_rows(p, u), out_rows(me_fs, u),
+            home_send.at[p, u], home_recv.at[me_fs, u], p, me_sp, me_tp,
         )
 
     def mass_out(p):
         return remote(
-            mass_ref.at[p], all_mass_ref.at[me_sp], msend.at[p], mrecv.at[me_sp], p, me_fs, me_tp
+            mass_ref.at[p], mass_in.at[me_sp], msend.at[p], mrecv.at[me_sp], p, me_fs, me_tp
         )
 
     def mine(p):
@@ -564,78 +581,99 @@
             barrier, inc=1, device_id={"sp": sp, "fs": fs, "tp": tp},
             device_id_type=pl.DeviceIdType.MESH,
         )
-    for load in loads:
+    for load in loads + out_loads:
         load.start()
-    for load in out_loads:
-        load.start()
+    for load in loads[:2]:
+        load.wait()
     pl.semaphore_wait(barrier, len(partners))
 
     @pl.when(home)
     def _():
-        for r in (3, 1, 2):
-            rows_home(r).start()
-        pltpu.make_async_copy(
-            piece_of(me_fs), x_ref.at[me_sp, me_fs, me_tp], in_recv.at[me_sp]
-        ).start()
+        for h in range(2):
+            for r in (1, 2, 3):
+                rows_home(r, h).start()
+            pltpu.make_async_copy(
+                piece_of(me_fs, h, 1), half_of(me_sp, me_fs, h), in_recv.at[me_sp, h]
+            ).start()
         pltpu.make_async_copy(shift_ref, rows_ref.at[me_sp], shz_recv.at[me_sp]).start()
 
     @pl.when(jnp.logical_not(home))
     def _():
-        for r in (3, 1, 2):
-            rows_out(r).start()
-        rows_on(0).start()
+        for h in range(2):
+            for r in (1, 2, 3):
+                rows_out(r, h).start()
         shift_on(0).start()
 
     for r in (1, 2, 3):
         shift_out(r).start()
 
-    def forward(r):
-        stay = columns[r] == me_sp
-
-        @pl.when(jnp.logical_not(stay))
+    def goes_at(r, stage):
+        target = columns[r]
+        place = me_sp + (me_sp < target).astype(jnp.int32)
+        return jnp.logical_and(target != me_sp, place == stage)
+
+    def forward_rows(stage):
+        @pl.when(goes_at(0, stage))
         def _():
-            landed(via.at[r - 1], via_recv.at[r - 1])
-            rows_on(r).start()
-            landed(via_shift.at[r - 1], sh_recv.at[r - 1])
+            for h in range(2):
+                rows_on(0, h).start()
+
+        for h in range(2):
+            for r in (1, 2, 3):
+
+                @pl.when(goes_at(r, stage))
+                def _():
+                    landed(via.at[r - 1, h], via_recv.at[r - 1, h])
+                    rows_on(r, h).start()
+
+    def forward_shift(r):
+        landed(via_shift.at[r - 1], sh_recv.at[r - 1])
+
+        @pl.when(columns[r] != me_sp)
+        def _():
             shift_on(r).start()
 
-        @pl.when(stay)
+        @pl.when(columns[r] == me_sp)
         def _():
-            landed(via_shift.at[r - 1], sh_recv.at[r - 1])
             pltpu.make_async_copy(
                 via_shift.at[r - 1], rows_ref.at[me_sp], shz_recv.at[me_sp]
             ).start()
 
-    for r in (1, 2, 3):
-        forward(r)
-    for give in out_gives:
-        give.start()
+    def forward_small():
+        for r in (1, 2, 3):
+            forward_shift(r)
+        for give in out_gives:
+            give.start()
 
     def arrive(p):
-        landed(x_ref.at[p, me_fs, me_tp], in_recv.at[p])
-        near_copy(p, 1).start()
-        near_copy(p, 2).start()
+        for h in range(2):
+            landed(half_of(p, me_fs, h), in_recv.at[p, h])
+        for k in range(2):
+            near_copy(p, 1, k).start()
+            near_copy(p, 2, k).start()
         across(p, 0).start()
 
-    def relay(p):
-        for r in (1, 2):
-            landed(x_ref.at[p, columns[r], me_tp], g_recv.at[p, r - 1])
-            half_copy(p, 3 - r).start()
-            across(p, r).start()
-
-    def gather_rest(p):
-        for r in (1, 2):
-            landed(
-                x_ref.at[p, columns[3], me_tp, pl.ds((r % 2) * half, half)], h_recv.at[p, r - 1]
-            )
-            across(p, 3 + r % 2).start()
+    def relay(p, r):
+        landed(half_of(p, columns[r], r - 1), g_recv.at[p, r - 1, 0])
+        half_copy(p, 3 - r).start()
+
+    def pass_across(p, r):
+        landed(half_of(p, columns[r], r % 2), g_recv.at[p, r - 1, 1])
+        across(p, r).start()
+
+    def pass_half(p, r):
+        landed(half_of(p, columns[3], r % 2), h_recv.at[p, r - 1])
+        across(p, 3 + r % 2).start()
 
     def complete(p):
         for r in range(5):
             crossed(p, r)
         landed(rows_ref.at[p], shz_recv.at[p])
 
+    head = me_fs * parts + me_tp
+
     def project_rows(p):
+        bias = bias_ref[:, pl.ds(pl.multiple_of(head * GLA_KEY, GLA_KEY), GLA_KEY)]
         here = pl.ds(pl.multiple_of(p * rows, rows), rows)
         halves = [x_ref[p, :, t].reshape(rows, width).astype(jnp.float32) for t in range(parts)]
         square = sum(jnp.sum(h * h, axis=-1, keepdims=True) for h in halves)
@@ -647,6 +685,7 @@
             ],
             axis=1,
         )
+        normed_s[...] = normed
         qk = nn(normed, jnp.concatenate([lq_ref[...], lk_ref[...]], axis=1)).astype(bf)
         q_s[here, :] = qk[:, :GLA_KEY]
         k_s[here, :] = qk[:, GLA_KEY:]
@@ -655,9 +694,13 @@
         sub = lax.broadcasted_iota(jnp.int32, (rows_ref.shape[1], 2 * GLA_KEY), 0)
         pick = jnp.where(sub == lane // GLA_KEY, 1.0, 0.0).astype(bf)
         shift = tn(rows_ref[p], pick)
-        gate = nn(normed, ld_ref[...]) + bias_ref[...] + shift[:, :GLA_KEY]
+        gate = nn(normed, ld_ref[...]) + bias + shift[:, :GLA_KEY]
         log_sig = jnp.minimum(gate, 0.0) - jnp.log1p(jnp.exp(-jnp.abs(gate)))
         dec_s[here, :] = log_sig * (1.0 / decay_tau) + shift[:, GLA_KEY:]
+
+    def project_soft(p):
+        here = pl.ds(pl.multiple_of(p * rows, rows), rows)
+        normed = normed_s[...]
         cos, sin = cos_ref[here, :], sin_ref[here, :]
         for w_ref, dst in ((sq_ref, a_s), (sk_ref, b_s)):
             wide = nn(normed, w_ref[...]).astype(bf).astype(jnp.float32)
@@ -693,7 +736,7 @@
         norm = lax.rsqrt(jnp.mean(raw * raw, axis=-1, keepdims=True) + norm_eps)
         mix_s[here, :GLA_VALUE] = (raw * norm * lgain_ref[...]).astype(bf)
 
-    lam = lam_ref[0]
+    heads_at = lax.broadcasted_iota(jnp.int32, lam_ref.shape, 1)
     rate = scale * float(np.log2(np.e))
     key_pos = lax.broadcasted_iota(jnp.int32, (rows, rows), 0)
     query_pos = lax.broadcasted_iota(jnp.int32, (rows, rows), 1)
@@ -714,6 +757,7 @@
             mass_ref[j, m : m + 1, :] = top * scale + jnp.log(total)
             pieces.append((mass, 1.0 / total))
         (one, one_rate), (two, two_rate) = pieces
+        lam = jnp.sum(jnp.where(heads_at == head, lam_ref[...], 0.0), axis=1, keepdims=True)
         two_rate = lam * two_rate
         raw = sum(
             tn((u * one_rate - w * two_rate).astype(bf), c_s[span, :])
@@ -728,64 +772,62 @@
 
         @pl.when(j == me_sp)
         def _():
-            pltpu.make_async_copy(mass_ref.at[j], all_mass_ref.at[j], mrecv.at[j]).start()
-
-    def mix_rows(j):
+            pltpu.make_async_copy(mass_ref.at[j], mass_in.at[j], mrecv.at[j]).start()
+
+    def advance_rows(j):
         for n in range(rows // CHUNK):
             advance(j * rows + n * CHUNK)
-        attend_rows(j)
-        mix_out(j).start()
-
-    def leave(j):
-        landed(omix_s.at[pl.ds(j * rows, rows)], mix_recv.at[j])
+
+    def leave(j, u):
+        if u == 0:
+            landed(omix_s.at[block_rows(j)], mix_recv.at[j])
 
         def turned(ref):
-            return jnp.concatenate(
-                [
-                    ref[pl.ds(pl.multiple_of(j * rows + c * piece, piece), piece), :]
-                    for c in columns
-                ],
-                axis=0,
-            )
+            starts = [pl.multiple_of(j * rows + c * piece + u * half, half) for c in columns]
+            return jnp.concatenate([ref[pl.ds(start, half), :] for start in starts], axis=0)
 
         full = nn(turned(mix_s), wout_ref[0]) + nn(turned(omix_s), wout_ref[1])
-        parted = [full[i * half : (i + 1) * half] for i in range(2 * count)]
-        first_x[j, 0] = parted[2].astype(bf)
-        first_x[j, 1] = parted[6].astype(bf)
-        first_y[j, 0] = parted[5].astype(bf)
-        first_y[j, 1] = parted[7].astype(bf)
-        own_s[j, 0] = parted[0]
-        own_s[j, 1] = parted[1]
-        later_s[j, 0] = parted[3]
-        later_s[j, 1] = parted[4]
-        first_out(j, 1).start()
-        first_out(j, 2).start()
-
-    def pass_on(j):
-        landed(got_x.at[j], f_recv.at[j, 0])
-        second_y[j] = (later_s[j, 1] + got_x[j, 1].astype(jnp.float32)).astype(bf)
-        second_out(j, 2).start()
-        landed(got_y.at[j], f_recv.at[j, 1])
-        second_x[j] = (later_s[j, 0] + got_y[j, 1].astype(jnp.float32)).astype(bf)
-        second_out(j, 1).start()
-
-    def finish(j):
-        landed(more_y.at[j], s_recv.at[j, 1])
-        final[j, pl.ds(0, half)] = (
-            own_s[j, 0] + got_x[j, 0].astype(jnp.float32) + more_y[j].astype(jnp.float32)
+        parted = [full[i * quarter : (i + 1) * quarter] for i in range(2 * count)]
+        first_x[j, u, 0] = parted[2].astype(bf)
+        first_x[j, u, 1] = parted[6].astype(bf)
+        first_y[j, u, 0] = parted[5].astype(bf)
+        first_y[j, u, 1] = parted[7].astype(bf)
+        own_s[j, u, 0] = parted[0]
+        own_s[j, u, 1] = parted[1]
+        later_s[j, u, 0] = parted[3]
+        later_s[j, u, 1] = parted[4]
+        first_out(j, u, 1).start()
+        first_out(j, u, 2).start()
+
+    def pass_above(j, u):
+        landed(got_x.at[j, u], f_recv.at[j, u, 0])
+        second_y[j, u] = (later_s[j, u, 1] + got_x[j, u, 1].astype(jnp.float32)).astype(bf)
+        second_out(j, u, 2).start()
+
+    def pass_beside(j, u):
+        landed(got_y.at[j, u], f_recv.at[j, u, 1])
+        second_x[j, u] = (later_s[j, u, 0] + got_y[j, u, 1].astype(jnp.float32)).astype(bf)
+        second_out(j, u, 1).start()
+
+    def finish(j, u):
+        landed(more_y.at[j, u], s_recv.at[j, u, 1])
+        landed(more_x.at[j, u], s_recv.at[j, u, 0])
+        final[j, pl.ds(u * half, quarter)] = (
+            own_s[j, u, 0] + got_x[j, u, 0].astype(jnp.float32) + more_y[j, u].astype(jnp.float32)
         ).astype(bf)
-        landed(more_x.at[j], s_recv.at[j, 0])
-        final[j, pl.ds(half, half)] = (
-            own_s[j, 1] + got_y[j, 0].astype(jnp.float32) + more_x[j].astype(jnp.float32)
+        final[j, pl.ds(u * half + quarter, quarter)] = (
+            own_s[j, u, 1] + got_y[j, u, 0].astype(jnp.float32) + more_x[j, u].astype(jnp.float32)
         ).astype(bf)
 
         @pl.when(jnp.logical_not(mine(j)))
         def _():
-            home_out(j).start()
+            home_out(j, u).start()
 
         @pl.when(mine(j))
         def _():
-            pltpu.make_async_copy(final.at[j], out_ref.at[me_fs], home_recv.at[me_fs]).start()
+            pltpu.make_async_copy(
+                final_rows(j, u), out_rows(me_fs, u), home_recv.at[me_fs, u]
+            ).start()
 
     def slot(i):
         if i == 0:
@@ -794,62 +836,113 @@
 
     state_s[...] = jnp.zeros_like(state_s)
     order = [slot(i) for i in range(planes)]
+    forward_rows(3)
+    forward_rows(1)
     arrive(order[0])
-    relay(order[0])
+    forward_small()
+    relay(order[0], 1)
+    relay(order[0], 2)
+    forward_rows(2)
+    pass_across(order[0], 1)
     arrive(order[1])
-    gather_rest(order[0])
+    pass_across(order[0], 2)
+    pass_half(order[0], 2)
+    arrive(order[3])
+    pass_half(order[0], 1)
     complete(order[0])
-    for load in loads:
+    relay(order[1], 1)
+    for load in loads[2:]:
         load.wait()
     project_rows(order[0])
-
-    relay(order[1])
+    relay(order[1], 2)
     arrive(order[2])
-    gather_rest(order[1])
+    pass_across(order[1], 1)
+    relay(order[3], 1)
+    relay(order[3], 2)
+    project_soft(order[0])
+    pass_half(order[1], 1)
+    pass_across(order[3], 2)
+    pass_half(order[1], 2)
+    pass_across(order[1], 2)
+    relay(order[2], 2)
+    relay(order[2], 1)
     complete(order[1])
     project_rows(order[1])
-    mix_rows(0)
-
-    relay(order[2])
-    arrive(order[3])
+    project_soft(order[1])
+    attend_rows(0)
+    pass_half(order[3], 1)
+    pass_across(order[3], 1)
+    pass_across(order[2], 1)
+    pass_half(order[3], 2)
+    pass_across(order[2], 2)
+    pass_half(order[2], 2)
+    pass_half(order[2], 1)
+    advance_rows(0)
+    mix_out(0).start()
+    complete(order[3])
+    complete(order[2])
+    project_rows(order[2])
+    project_soft(order[2])
+    advance_rows(1)
     for load in out_loads:
         load.wait()
     for give in out_gives:
         give.wait_recv()
-    leave(0)
-    gather_rest(order[2])
-    complete(order[2])
-    project_rows(order[2])
-    mix_rows(1)
-
-    relay(order[3])
-    leave(1)
-    pass_on(0)
-    gather_rest(order[3])
-    complete(order[3])
+    leave(0, 0)
+    leave(0, 1)
+    attend_rows(1)
+    mix_out(1).start()
     project_rows(order[3])
-    mix_rows(2)
-    finish(0)
-    pass_on(1)
-    leave(2)
-    mix_rows(3)
-    finish(1)
-    pass_on(2)
-    leave(3)
-    finish(2)
-    pass_on(3)
-    finish(3)
-
+    project_soft(order[3])
+    leave(1, 0)
+    advance_rows(2)
+    leave(1, 1)
+    pass_above(0, 0)
+    pass_beside(0, 0)
+    attend_rows(3)
+    pass_beside(0, 1)
+    advance_rows(3)
+    mix_out(3).start()
+    attend_rows(2)
+    mix_out(2).start()
+    pass_above(1, 1)
+    pass_beside(1, 1)
+    leave(3, 0)
+    leave(2, 0)
+    leave(3, 1)
+    pass_beside(3, 0)
+    pass_above(3, 0)
+    pass_above(0, 1)
+    pass_beside(2, 0)
+    pass_above(2, 0)
+    pass_above(1, 0)
+    leave(2, 1)
+    finish(1, 1)
+    pass_beside(1, 0)
+    pass_above(3, 1)
+    finish(3, 0)
+    pass_beside(3, 1)
+    finish(0, 1)
+    finish(2, 0)
+    pass_above(2, 1)
+    finish(0, 0)
+    finish(1, 0)
+    pass_beside(2, 1)
+    finish(3, 1)
+    finish(2, 1)
     for p in range(planes):
-        landed(all_mass_ref.at[p], mrecv.at[p])
+        landed(mass_in.at[p], mrecv.at[p])
+        all_mass_ref[:, p, :] = mass_in[p]
         mix_out(p).wait_send()
         for r in range(5):
             across(p, r).wait_send()
         for r in (1, 2):
-            near_copy(p, r).wait_send()
+            near_copy(p, r, 0).wait_send()
+            near_copy(p, r, 1).wait_send()
             half_copy(p, r).wait_send()
-            first_out(p, r).wait_send()
-            second_out(p, r).wait_send()
+            for u in range(2):
+                first_out(p, u, r).wait_send()
+                second_out(p, u, r).wait_send()
 
         @pl.when(p != me_sp)
         def _():
@@ -857,27 +950,32 @@
 
         @pl.when(jnp.logical_not(mine(p)))
         def _():
-            home_out(p).wait_send()
+            home_out(p, 0).wait_send()
+            home_out(p, 1).wait_send()
 
     for give in out_gives:
         give.wait_send()
 
     @pl.when(jnp.logical_not(home))
     def _():
-        rows_on(0).wait_send()
+        for h in range(2):
+            rows_on(0, h).wait_send()
         shift_on(0).wait_send()
 
     for r in (1, 2, 3):
-        rows_out(r).wait_send()
+        for h in range(2):
+            rows_out(r, h).wait_send()
         shift_out(r).wait_send()
 
         @pl.when(columns[r] != me_sp)
         def _():
-            rows_on(r).wait_send()
+            for h in range(2):
+                rows_on(r, h).wait_send()
             shift_on(r).wait_send()
 
     for c in range(count):
-        landed(out_ref.at[c], home_recv.at[c])
+        for u in range(2):
+            landed(out_rows(c, u), home_recv.at[c, u])
 
 
 def turned_shards(
@@ -902,17 +1000,15 @@
     rows, width = tokens.shape[1:]
     planes, count, parts = sizes["sp"], sizes["fs"], sizes["tp"]
     piece = rows // count
-    half = piece // 2
+    half, quarter = piece // 2, piece // 4
     length = planes * rows
-    head = lax.axis_index("fs") * parts + lax.axis_index("tp")
     bf, f32 = jnp.bfloat16, jnp.float32
     vmem = pl.BlockSpec(memory_space=pltpu.VMEM)
     dma = pltpu.SemaphoreType.DMA
-    shift = jnp.pad(decay_shift[:, 0, :], ((0, 14), (0, 0)))
-    own_lambda = lax.dynamic_slice_in_dim(soft_lambda, head, 1, 0)
-    own_bias = lax.dynamic_slice_in_dim(decay_bias, head * GLA_KEY, GLA_KEY, 0)[None]
     cos, sin = turn_tables(length)
     weights = (
+        tokens[0], decay_shift[:, 0, :], norm_gain[None], decay_bias[None], soft_lambda[None],
+        lin_gain[None], soft_gain[None],
         lin_query, lin_key, lin_decay, lin_value, jnp.asarray(cos), jnp.asarray(sin),
         soft_query, soft_key, soft_value, jnp.asarray(level_sums(CHUNK), bf),
     )
@@ -920,18 +1016,16 @@
         functools.partial(layer_kernel, sizes),
         out_shape=(
             jax.ShapeDtypeStruct((count, piece, width), bf),
-            jax.ShapeDtypeStruct((planes, 2, rows), f32),
+            jax.ShapeDtypeStruct((2, planes, rows), f32),
         ),
-        in_specs=[vmem] * 4
-        + [pl.BlockSpec(memory_space=pltpu.SMEM)]
-        + [vmem] * 2
-        + [pl.BlockSpec(memory_space=pl.ANY)] * (WEIGHTS + 2),
+        in_specs=[pl.BlockSpec(memory_space=pl.ANY)] * (WEIGHTS + 2),
         out_specs=[vmem] * 2,
         scratch_shapes=[pltpu.VMEM(w.shape, w.dtype) for w in weights]
         + [
             pltpu.VMEM((2, GLA_VALUE + DIFF_VALUE, width), bf),
             pltpu.VMEM((planes, count, parts, piece, width), bf),
-            pltpu.VMEM((planes, 16, rows), bf),
+            pltpu.VMEM((planes, 2, rows), bf),
+            pltpu.VMEM((rows, parts * width), bf),
             pltpu.VMEM((length, GLA_KEY), bf),
             pltpu.VMEM((length, GLA_KEY), bf),
             pltpu.VMEM((length, GLA_VALUE), bf),
@@ -943,36 +1037,36 @@
             pltpu.VMEM((length, GLA_VALUE + DIFF_VALUE), bf),
             pltpu.VMEM((length, GLA_VALUE + DIFF_VALUE), bf),
             pltpu.VMEM((planes, 2, rows), f32),
-            pltpu.VMEM((count - 1, piece, width), bf),
-            pltpu.VMEM((count - 1, 16, rows), bf),
-            pltpu.VMEM((planes, 2, half, width), f32),
-            pltpu.VMEM((planes, 2, half, width), f32),
-            pltpu.VMEM((planes, 2, half, width), bf),
-            pltpu.VMEM((planes, 2, half, width), bf),
-            pltpu.VMEM((planes, 2, half, width), bf),
-            pltpu.VMEM((planes, 2, half, width), bf),
-            pltpu.VMEM((planes, half, width), bf),
-            pltpu.VMEM((planes, half, width), bf),
-            pltpu.VMEM((planes, half, width), bf),
-            pltpu.VMEM((planes, half, width), bf),
+            pltpu.VMEM((planes, 2, rows), f32),
+            pltpu.VMEM((count - 1, 2, half, width), bf),
+            pltpu.VMEM((count - 1, 2, rows), bf),
+            pltpu.VMEM((planes, 2, 2, quarter, width), f32),
+            pltpu.VMEM((planes, 2, 2, quarter, width), f32),
+            pltpu.VMEM((planes, 2, 2, quarter, width), bf),
+            pltpu.VMEM((planes, 2, 2, quarter, width), bf),
+            pltpu.VMEM((planes, 2, 2, quarter, width), bf),
+            pltpu.VMEM((planes, 2, 2, quarter, width), bf),
+            pltpu.VMEM((planes, 2, quarter, width), bf),
+            pltpu.VMEM((planes, 2, quarter, width), bf),
+            pltpu.VMEM((planes, 2, quarter, width), bf),
+            pltpu.VMEM((planes, 2, quarter, width), bf),
             pltpu.VMEM((planes, piece, width), bf),
             dma((WEIGHTS,)), dma((2,)), dma((2,)), dma((2,)),
+            dma((count - 1, 2)), dma((count - 1, 2)), dma((count, 2)), dma((planes, 2)),
             dma((count - 1,)), dma((count - 1,)), dma((count,)), dma((planes,)),
-            dma((count - 1,)), dma((count - 1,)), dma((count,)), dma((planes,)),
-            dma((planes, 2)), dma((planes, 2)), dma((planes, 2)), dma((planes, 2)),
+            dma((planes, 2, 2)), dma((planes, 2, 2)), dma((planes, 2)), dma((planes, 2)),
             dma((planes, 5)), dma((planes, 5)), dma((planes,)), dma((planes,)),
-            dma((planes, 2)), dma((planes, 2)), dma((planes, 2)), dma((planes, 2)),
-            dma((planes,)), dma((count,)), dma((planes,)), dma((planes,)),
+            dma((planes, 2, 2)), dma((planes, 2, 2)), dma((planes, 2, 2)), dma((planes, 2, 2)),
+            dma((planes, 2)), dma((count, 2)), dma((planes,)), dma((planes,)),
         ],
         compiler_params=pltpu.CompilerParams(
             has_side_effects=True, collective_id=0, vmem_limit_bytes=60 * 1024 * 1024
         ),
         name="whole_layer",
     )(
-        tokens[0], shift, norm_gain[None], own_bias, own_lambda, lin_gain[None], soft_gain[None],
         *weights, lin_out, soft_out,
     )
-    return mixed.reshape(1, rows, width), all_mass.transpose(1, 0, 2)[None]
+    return mixed.reshape(1, rows, width), all_mass[None]
 
 
 def solution(mesh):

time: 89.6 us -> 74.8 us (0.83)
  the two profiles are of different devices: /device:TPU:26 before, /device:TPU:16 now
where the time goes in v2:
time: 74.8 us; the launch traced here: 74.6 us
  Pallas kernels  71.5 us (96%)
  local copies, waits for them, and re-layouts  2.48 us (3%)
    pallas_call x1, Pallas kernels, turned_shards(): pl.pallas_call(functools.partial(layer_kernel, sizes), out_shape=(jax.Sha...  71.5 us
    unnamed x4, local copies, waits for them, and re-layouts  2.48 us

profile of v2, /device:TPU:16, one launch (start us, length us, event | category | flops | bytes accessed | tf_op | source)
XLA Modules:
  0.0 74.6 jit_solution(18213454136594394319)
XLA Ops:
  0.6 71.5 %whole_layer.1 = (bf16[4,64,1024]{2,1,0:T(8,128)(2,1)}, f32[2,4,256]{2,1,0:T(4,128)}) custom-call(bf16[256,1024]{1,0:T(8,128)(2,1)} %bitcast.9, bf16[2,256]{1,0:T(2,128)(2,1)} %bitcast.14, f32[1,2048]{1,0:T(1,128)} %bitcast.11, f32[1,1024]{1,0:T(1,128)} %bitcast.13, f32[1,8]{1,0:T(1,128)} %bitcast.17, f32[1,256]{1,0:T(1,128)} %bitcast.15, ...), custom_call_target="tpu_custom_call" | custom-call | tf_op jit(solution)/shard_map/whole_layer/pallas_call | solution.py:1015
  72.1 0.0 copy-start
  72.1 1.9 %copy.23 = bf16[1,256,1024]{2,1,0:T(8,128)(2,1)} copy(bf16[1,256,1024]{2,1,0:T(8,128)(2,1)} %bitcast.10) | data formatting | bytes 1048576
  74.0 0.0 copy-done
  74.0 0.6 copy.24
Async XLA Ops:
  72.1 1.9 %copy-start = (f32[2,4,256]{2,1,0:T(4,128)S(1)}, f32[2,4,256]{2,1,0:T(4,128)}, u32[]{:S(2)}) copy-start(f32[2,4,256]{2,1,0:T(4,128)} %get-tuple-element.5) | copy-start | bytes 24580

commit v3 on v2

--- a/solution.py
+++ b/solution.py
@@ -414,7 +414,7 @@
         wsem, osem, wo_send, wo_recv, sc_send, via_recv, z_send, in_recv,
         sh_send, sh_recv, shz_send, shz_recv,
         g_send, g_recv, h_send, h_recv, ac_send, ac_recv, mix_send, mix_recv,
-        f_send, f_recv, s_send, s_recv, home_send, home_recv, msend, mrecv,
+        ready, f_send, f_recv, s_send, s_recv, home_send, home_recv, msend, mrecv,
     ) = refs[2 * WEIGHTS + 4 :]
     (
         tok_ref, shift_ref, gain_ref, bias_ref, lam_ref, lgain_ref, sgain_ref,
@@ -573,25 +573,70 @@
         for i, f in enumerate((lo_far, so_far))
     ]
 
+    def tell(sem, sp, fs, tp):
+        pl.semaphore_signal(
+            sem, inc=1, device_id={"sp": sp, "fs": fs, "tp": tp},
+            device_id_type=pl.DeviceIdType.MESH,
+        )
+
     barrier = pltpu.get_barrier_semaphore()
-    partners = [(me_sp, c, me_tp) for c in columns[1:]] + [(me_sp, me_fs, other)]
-    partners += [(lax.rem(me_sp + d, planes), me_fs, me_tp) for d in range(1, planes)]
-    for sp, fs, tp in partners:
-        pl.semaphore_signal(
-            barrier, inc=1, device_id={"sp": sp, "fs": fs, "tp": tp},
-            device_id_type=pl.DeviceIdType.MESH,
-        )
+    below, over = me_sp > 0, me_sp < planes - 1
+    for c in columns[1:3]:
+        tell(barrier, me_sp, c, me_tp)
+    tell(barrier, me_sp, me_fs, other)
+
+    @pl.when(below)
+    def _():
+        tell(barrier, me_sp - 1, me_fs, me_tp)
+
+    @pl.when(over)
+    def _():
+        tell(barrier, me_sp + 1, me_fs, me_tp)
+
     for load in loads + out_loads:
         load.start()
     for load in loads[:2]:
         load.wait()
-    pl.semaphore_wait(barrier, len(partners))
+    pl.semaphore_wait(barrier, 3 + below.astype(jnp.int32) + over.astype(jnp.int32))
+
+    tell(ready.at[0], me_sp, columns[2], me_tp)
+
+    @pl.when(jnp.logical_and(below, over))
+    def _():
+        tell(ready.at[1], me_sp - 1, me_fs, me_tp)
+        tell(ready.at[2], me_sp + 1, me_fs, me_tp)
+
+    def far_ready():
+        for steps in range(2, planes):
+            up, down = me_sp + steps < planes, me_sp >= steps
+
+            @pl.when(up)
+            def _():
+                pl.semaphore_wait(ready.at[2 * steps - 3], 1)
+
+            @pl.when(down)
+            def _():
+                pl.semaphore_wait(ready.at[2 * steps - 2], 1)
+
+            if steps + 1 < planes:
+
+                @pl.when(jnp.logical_and(up, below))
+                def _():
+                    tell(ready.at[2 * steps - 1], me_sp - 1, me_fs, me_tp)
+
+                @pl.when(jnp.logical_and(down, over))
+                def _():
+                    tell(ready.at[2 * steps], me_sp + 1, me_fs, me_tp)
+
 
     @pl.when(home)
     def _():
         for h in range(2):
-            for r in (1, 2, 3):
+            for r in (1, 2):
                 rows_home(r, h).start()
+            if h == 0:
+                pl.semaphore_wait(ready.at[0], 1)
+            rows_home(3, h).start()
             pltpu.make_async_copy(
                 piece_of(me_fs, h, 1), half_of(me_sp, me_fs, h), in_recv.at[me_sp, h]
             ).start()
@@ -600,9 +645,17 @@
     @pl.when(jnp.logical_not(home))
     def _():
         for h in range(2):
-            for r in (1, 2, 3):
+            for r in (1, 2):
                 rows_out(r, h).start()
+            if h == 0:
+                pl.semaphore_wait(ready.at[0], 1)
+            rows_out(3, h).start()
+        far_ready()
         shift_on(0).start()
+
+    @pl.when(home)
+    def _():
+        far_ready()
 
     for r in (1, 2, 3):
         shift_out(r).start()
@@ -836,99 +889,99 @@
 
     state_s[...] = jnp.zeros_like(state_s)
     order = [slot(i) for i in range(planes)]
+    forward_rows(1)
     forward_rows(3)
-    forward_rows(1)
     arrive(order[0])
     forward_small()
     relay(order[0], 1)
     relay(order[0], 2)
     forward_rows(2)
-    pass_across(order[0], 1)
     arrive(order[1])
     pass_across(order[0], 2)
     pass_half(order[0], 2)
+    pass_across(order[0], 1)
     arrive(order[3])
     pass_half(order[0], 1)
+    relay(order[1], 2)
+    relay(order[1], 1)
     complete(order[0])
-    relay(order[1], 1)
     for load in loads[2:]:
         load.wait()
     project_rows(order[0])
-    relay(order[1], 2)
     arrive(order[2])
+    project_soft(order[0])
+    relay(order[3], 2)
     pass_across(order[1], 1)
     relay(order[3], 1)
-    relay(order[3], 2)
-    project_soft(order[0])
+    pass_across(order[1], 2)
     pass_half(order[1], 1)
-    pass_across(order[3], 2)
     pass_half(order[1], 2)
-    pass_across(order[1], 2)
     relay(order[2], 2)
     relay(order[2], 1)
     complete(order[1])
     project_rows(order[1])
     project_soft(order[1])
+    pass_across(order[3], 1)
+    pass_across(order[3], 2)
+    pass_half(order[3], 1)
+    pass_across(order[2], 2)
+    pass_half(order[3], 2)
+    pass_across(order[2], 1)
     attend_rows(0)
-    pass_half(order[3], 1)
-    pass_across(order[3], 1)
-    pass_across(order[2], 1)
-    pass_half(order[3], 2)
-    pass_across(order[2], 2)
     pass_half(order[2], 2)
     pass_half(order[2], 1)
     advance_rows(0)
     mix_out(0).start()
-    complete(order[3])
     complete(order[2])
     project_rows(order[2])
     project_soft(order[2])
+    complete(order[3])
     advance_rows(1)
+    attend_rows(1)
+    mix_out(1).start()
     for load in out_loads:
         load.wait()
     for give in out_gives:
         give.wait_recv()
     leave(0, 0)
-    leave(0, 1)
-    attend_rows(1)
-    mix_out(1).start()
     project_rows(order[3])
     project_soft(order[3])
+    advance_rows(2)
     leave(1, 0)
-    advance_rows(2)
+    attend_rows(2)
+    mix_out(2).start()
+    leave(0, 1)
+    advance_rows(3)
+    leave(2, 0)
+    leave(2, 1)
+    attend_rows(3)
+    mix_out(3).start()
+    pass_above(1, 0)
     leave(1, 1)
+    leave(3, 0)
+    pass_beside(2, 0)
+    pass_beside(1, 0)
+    pass_above(2, 0)
+    leave(3, 1)
     pass_above(0, 0)
     pass_beside(0, 0)
-    attend_rows(3)
-    pass_beside(0, 1)
-    advance_rows(3)
-    mix_out(3).start()
-    attend_rows(2)
-    mix_out(2).start()
-    pass_above(1, 1)
-    pass_beside(1, 1)
-    leave(3, 0)
-    leave(2, 0)
-    leave(3, 1)
     pass_beside(3, 0)
     pass_above(3, 0)
+    finish(2, 0)
     pass_above(0, 1)
-    pass_beside(2, 0)
-    pass_above(2, 0)
-    pass_above(1, 0)
-    leave(2, 1)
+    pass_beside(0, 1)
+    pass_above(1, 1)
+    finish(1, 0)
+    pass_beside(3, 1)
+    pass_beside(1, 1)
+    pass_above(3, 1)
+    pass_beside(2, 1)
+    finish(0, 0)
+    pass_above(2, 1)
+    finish(3, 0)
+    finish(0, 1)
+    finish(3, 1)
     finish(1, 1)
-    pass_beside(1, 0)
-    pass_above(3, 1)
-    finish(3, 0)
-    pass_beside(3, 1)
-    finish(0, 1)
-    finish(2, 0)
-    pass_above(2, 1)
-    finish(0, 0)
-    finish(1, 0)
-    pass_beside(2, 1)
-    finish(3, 1)
     finish(2, 1)
     for p in range(planes):
         landed(mass_in.at[p], mrecv.at[p])
@@ -1019,7 +1072,7 @@
             jax.ShapeDtypeStruct((2, planes, rows), f32),
         ),
         in_specs=[pl.BlockSpec(memory_space=pl.ANY)] * (WEIGHTS + 2),
-        out_specs=[vmem] * 2,
+        out_specs=[pl.BlockSpec(memory_space=pl.ANY), vmem],
         scratch_shapes=[pltpu.VMEM(w.shape, w.dtype) for w in weights]
         + [
             pltpu.VMEM((2, GLA_VALUE + DIFF_VALUE, width), bf),
@@ -1056,6 +1109,7 @@
             dma((count - 1,)), dma((count - 1,)), dma((count,)), dma((planes,)),
             dma((planes, 2, 2)), dma((planes, 2, 2)), dma((planes, 2)), dma((planes, 2)),
             dma((planes, 5)), dma((planes, 5)), dma((planes,)), dma((planes,)),
+            pltpu.SemaphoreType.REGULAR((2 * planes - 3,)),
             dma((planes, 2, 2)), dma((planes, 2, 2)), dma((planes, 2, 2)), dma((planes, 2, 2)),
             dma((planes, 2)), dma((count, 2)), dma((planes,)), dma((planes,)),
         ],

time: 74.8 us -> 73.5 us (0.983)
  Pallas kernels: 71.5 us -> 70.2 us
    pallas_call x1, Pallas kernels: 71.5 us -> 70.2 us  [turned_shards(): pl.pallas_call(functools.partial(layer_kernel, sizes), out_shape=(jax.Sha...]
where the time goes in v3:
time: 73.5 us; the launch traced here: 73.3 us
  Pallas kernels  70.2 us (96%)
  local copies, waits for them, and re-layouts  2.48 us (3%)
    pallas_call x1, Pallas kernels, turned_shards(): pl.pallas_call(functools.partial(layer_kernel, sizes), out_shape=(jax.Sha...  70.2 us
    unnamed x4, local copies, waits for them, and re-layouts  2.48 us

profile of v3, /device:TPU:16, one launch (start us, length us, event | category | flops | bytes accessed | tf_op | source)
XLA Modules:
  0.0 73.3 jit_solution(6665791977219793927)
XLA Ops:
  0.6 70.2 %whole_layer.1 = (bf16[4,64,1024]{2,1,0:T(8,128)(2,1)}, f32[2,4,256]{2,1,0:T(4,128)}) custom-call(bf16[256,1024]{1,0:T(8,128)(2,1)} %bitcast.9, bf16[2,256]{1,0:T(2,128)(2,1)} %bitcast.14, f32[1,2048]{1,0:T(1,128)} %bitcast.11, f32[1,1024]{1,0:T(1,128)} %bitcast.13, f32[1,8]{1,0:T(1,128)} %bitcast.17, f32[1,256]{1,0:T(1,128)} %bitcast.15, ...), custom_call_target="tpu_custom_call" | custom-call | tf_op jit(solution)/shard_map/whole_layer/pallas_call | solution.py:1068
  70.8 0.0 copy-start
  70.9 1.9 %copy.23 = bf16[1,256,1024]{2,1,0:T(8,128)(2,1)} copy(bf16[1,256,1024]{2,1,0:T(8,128)(2,1)} %bitcast.10) | data formatting | bytes 1048576
  72.7 0.0 copy-done
  72.7 0.6 copy.24
Async XLA Ops:
  70.8 1.9 %copy-start = (f32[2,4,256]{2,1,0:T(4,128)S(1)}, f32[2,4,256]{2,1,0:T(4,128)}, u32[]{:S(2)}) copy-start(f32[2,4,256]{2,1,0:T(4,128)} %get-tuple-element.5) | copy-start | bytes 24580

commit v4 on v3

--- a/solution.py
+++ b/solution.py
@@ -408,7 +408,7 @@
     out_ref, all_mass_ref = refs[WEIGHTS + 2 : WEIGHTS + 4]
     near = refs[WEIGHTS + 4 : 2 * WEIGHTS + 4]
     (
-        wout_ref, x_ref, rows_ref, normed_s, q_s, k_s, v_s, dec_s, a_s, b_s, c_s, state_s, mix_s, omix_s,
+        lqkd_ref, wout_ref, x_ref, rows_ref, normed_s, factor_s, q_s, k_s, v_s, dec_s, a_s, b_s, c_s, state_s, mix_s, omix_s,
         mass_ref, mass_in, via, via_shift, own_s, later_s, first_x, first_y, got_x, got_y,
         second_x, second_y, more_x, more_y, final,
         wsem, osem, wo_send, wo_recv, sc_send, via_recv, z_send, in_recv,
@@ -418,7 +418,7 @@
     ) = refs[2 * WEIGHTS + 4 :]
     (
         tok_ref, shift_ref, gain_ref, bias_ref, lam_ref, lgain_ref, sgain_ref,
-        lq_ref, lk_ref, ld_ref, lv_ref, cos_ref, sin_ref, sq_ref, sk_ref, sv_ref, span_ref,
+        _, _, _, lv_ref, cos_ref, sin_ref, sq_ref, sk_ref, sv_ref, span_ref,
     ) = near
     planes, count, parts, piece, width = x_ref.shape
     rows = count * piece
@@ -557,7 +557,9 @@
     def own_cols(t):
         return pl.ds(pl.multiple_of(t * width, width), width)
 
-    loads = [pltpu.make_async_copy(f, n, wsem.at[i]) for i, (f, n) in enumerate(zip(far, near))]
+    packed = [lqkd_ref.at[:, pl.ds(i * GLA_KEY, GLA_KEY)] for i in range(3)]
+    targets = list(near[:7]) + packed + list(near[10:])
+    loads = [pltpu.make_async_copy(f, n, wsem.at[i]) for i, (f, n) in enumerate(zip(far, targets))]
     depth = lo_far.shape[0]
     out_loads = [
         pltpu.make_async_copy(
@@ -729,52 +731,54 @@
         bias = bias_ref[:, pl.ds(pl.multiple_of(head * GLA_KEY, GLA_KEY), GLA_KEY)]
         here = pl.ds(pl.multiple_of(p * rows, rows), rows)
         halves = [x_ref[p, :, t].reshape(rows, width).astype(jnp.float32) for t in range(parts)]
-        square = sum(jnp.sum(h * h, axis=-1, keepdims=True) for h in halves)
-        factor = lax.rsqrt(square / (parts * width) + norm_eps)
-        normed = jnp.concatenate(
+        scaled = jnp.concatenate(
             [
-                (h * factor * gain_ref[:, t * width : (t + 1) * width]).astype(bf)
+                (h * gain_ref[:, t * width : (t + 1) * width]).astype(bf)
                 for t, h in enumerate(halves)
             ],
             axis=1,
         )
-        normed_s[...] = normed
-        qk = nn(normed, jnp.concatenate([lq_ref[...], lk_ref[...]], axis=1)).astype(bf)
-        q_s[here, :] = qk[:, :GLA_KEY]
-        k_s[here, :] = qk[:, GLA_KEY:]
-        v_s[here, :] = nn(normed, lv_ref[...]).astype(bf)
+        normed_s[...] = scaled
+        square = sum(jnp.sum(h * h, axis=-1, keepdims=True) for h in halves)
+        factor = lax.rsqrt(square / (parts * width) + norm_eps)
+        factor_s[...] = jnp.broadcast_to(factor, factor_s.shape)
+        qkd = nn(scaled, lqkd_ref[...])
+        q_s[here, :] = (qkd[:, :GLA_KEY] * factor).astype(bf)
+        k_s[here, :] = (qkd[:, GLA_KEY : 2 * GLA_KEY] * factor).astype(bf)
+        v_s[here, :] = (nn(scaled, lv_ref[...]) * factor).astype(bf)
         lane = lax.broadcasted_iota(jnp.int32, (rows_ref.shape[1], 2 * GLA_KEY), 1)
         sub = lax.broadcasted_iota(jnp.int32, (rows_ref.shape[1], 2 * GLA_KEY), 0)
         pick = jnp.where(sub == lane // GLA_KEY, 1.0, 0.0).astype(bf)
         shift = tn(rows_ref[p], pick)
-        gate = nn(normed, ld_ref[...]) + bias + shift[:, :GLA_KEY]
+        gate = qkd[:, 2 * GLA_KEY :] * factor + bias + shift[:, :GLA_KEY]
         log_sig = jnp.minimum(gate, 0.0) - jnp.log1p(jnp.exp(-jnp.abs(gate)))
         dec_s[here, :] = log_sig * (1.0 / decay_tau) + shift[:, GLA_KEY:]
 
     def project_soft(p):
         here = pl.ds(pl.multiple_of(p * rows, rows), rows)
-        normed = normed_s[...]
+        scaled = normed_s[...]
+        factor = factor_s[...]
         cos, sin = cos_ref[here, :], sin_ref[here, :]
         for w_ref, dst in ((sq_ref, a_s), (sk_ref, b_s)):
-            wide = nn(normed, w_ref[...]).astype(bf).astype(jnp.float32)
+            wide = nn(scaled, w_ref[...])
             for m in range(2):
-                one = wide[:, m * DIFF_HEAD : (m + 1) * DIFF_HEAD]
+                one = wide[:, m * DIFF_HEAD : (m + 1) * DIFF_HEAD] * factor
+                one = one.astype(bf).astype(jnp.float32)
                 turned = one * cos + pltpu.roll(one, DIFF_HEAD // 2, 1) * sin
                 dst[here, m * DIFF_HEAD : (m + 1) * DIFF_HEAD] = turned.astype(bf)
-        c_s[here, :] = nn(normed, sv_ref[...]).astype(bf)
+        wide = nn(scaled, sv_ref[...])
+        for m in range(2):
+            lanes = slice(m * DIFF_HEAD, (m + 1) * DIFF_HEAD)
+            c_s[here, lanes] = (wide[:, lanes] * factor).astype(bf)
 
     levels = CHUNK.bit_length() - 1
     row = lax.broadcasted_iota(jnp.int32, (CHUNK, CHUNK), 0)
     col = lax.broadcasted_iota(jnp.int32, (CHUNK, CHUNK), 1)
     apart = row ^ col
 
-    def advance(first):
+    def advance(first, factors):
         here = pl.ds(first, CHUNK)
         query, key, value = q_s[here, :].astype(jnp.float32), k_s[here, :].astype(jnp.float32), v_s[here, :]
-        decay = dec_s[here, :]
-        high = decay.astype(bf)
-        low = (decay - high.astype(jnp.float32)).astype(bf)
-        factors = jnp.exp(nn(span_ref[...], jnp.concatenate([high, low], axis=0)))
         scores = nt(q_s[here, :], k_s[here, :])
         for level in range(levels):
             factor = factors[level * CHUNK : (level + 1) * CHUNK]
@@ -828,8 +832,15 @@
             pltpu.make_async_copy(mass_ref.at[j], mass_in.at[j], mrecv.at[j]).start()
 
     def advance_rows(j):
-        for n in range(rows // CHUNK):
-            advance(j * rows + n * CHUNK)
+        chunks = rows // CHUNK
+        decay = jnp.concatenate(
+            [dec_s[pl.ds(j * rows + n * CHUNK, CHUNK), :] for n in range(chunks)], axis=1
+        )
+        high = decay.astype(bf)
+        low = (decay - high.astype(jnp.float32)).astype(bf)
+        factors = jnp.exp(nn(span_ref[...], jnp.concatenate([high, low], axis=0)))
+        for n in range(chunks):
+            advance(j * rows + n * CHUNK, factors[:, n * GLA_KEY : (n + 1) * GLA_KEY])
 
     def leave(j, u):
         if u == 0:
@@ -1073,12 +1084,17 @@
         ),
         in_specs=[pl.BlockSpec(memory_space=pl.ANY)] * (WEIGHTS + 2),
         out_specs=[pl.BlockSpec(memory_space=pl.ANY), vmem],
-        scratch_shapes=[pltpu.VMEM(w.shape, w.dtype) for w in weights]
+        scratch_shapes=[
+            pltpu.VMEM((16, 128) if 7 <= i < 10 else w.shape, w.dtype)
+            for i, w in enumerate(weights)
+        ]
         + [
+            pltpu.VMEM((lin_query.shape[0], 3 * GLA_KEY), bf),
             pltpu.VMEM((2, GLA_VALUE + DIFF_VALUE, width), bf),
             pltpu.VMEM((planes, count, parts, piece, width), bf),
             pltpu.VMEM((planes, 2, rows), bf),
             pltpu.VMEM((rows, parts * width), bf),
+            pltpu.VMEM((rows, DIFF_HEAD), f32),
             pltpu.VMEM((length, GLA_KEY), bf),
             pltpu.VMEM((length, GLA_KEY), bf),
             pltpu.VMEM((length, GLA_VALUE), bf),

time: 73.5 us -> 72.3 us (0.984)
  Pallas kernels: 70.2 us -> 69 us
    pallas_call x1, Pallas kernels: 70.2 us -> 69 us  [turned_shards(): pl.pallas_call(functools.partial(layer_kernel, sizes), out_shape=(jax.Sha...]
where the time goes in v4:
time: 72.3 us; the launch traced here: 72.1 us
  Pallas kernels  69 us (95%)
  local copies, waits for them, and re-layouts  2.48 us (3%)
    pallas_call x1, Pallas kernels, turned_shards(): pl.pallas_call(functools.partial(layer_kernel, sizes), out_shape=(jax.Sha...  69 us
    unnamed x4, local copies, waits for them, and re-layouts  2.48 us

profile of v4, /device:TPU:16, one launch (start us, length us, event | category | flops | bytes accessed | tf_op | source)
XLA Modules:
  0.0 72.1 jit_solution(295129156673108182)
XLA Ops:
  0.6 69.0 %whole_layer.1 = (bf16[4,64,1024]{2,1,0:T(8,128)(2,1)}, f32[2,4,256]{2,1,0:T(4,128)}) custom-call(bf16[256,1024]{1,0:T(8,128)(2,1)} %bitcast.9, bf16[2,256]{1,0:T(2,128)(2,1)} %bitcast.14, f32[1,2048]{1,0:T(1,128)} %bitcast.11, f32[1,1024]{1,0:T(1,128)} %bitcast.13, f32[1,8]{1,0:T(1,128)} %bitcast.17, f32[1,256]{1,0:T(1,128)} %bitcast.15, ...), custom_call_target="tpu_custom_call" | custom-call | tf_op jit(solution)/shard_map/whole_layer/pallas_call | solution.py:1079
  69.6 0.0 copy-start
  69.6 1.9 %copy.23 = bf16[1,256,1024]{2,1,0:T(8,128)(2,1)} copy(bf16[1,256,1024]{2,1,0:T(8,128)(2,1)} %bitcast.10) | data formatting | bytes 1048576
  71.5 0.0 copy-done
  71.5 0.6 copy.24
Async XLA Ops:
  69.6 1.9 %copy-start = (f32[2,4,256]{2,1,0:T(4,128)S(1)}, f32[2,4,256]{2,1,0:T(4,128)}, u32[]{:S(2)}) copy-start(f32[2,4,256]{2,1,0:T(4,128)} %get-tuple-element.5) | copy-start | bytes 24580
